TPU v7x, 256 devices: a whole 4x4x8 slice. The times are simulated.
256 devices in a mesh: sp: 16 (over y, x), tp: 16 (over z, core).
Axes of the slice: x: 4, y: 4, z: 8, core: 2. Of those that a mesh axis runs over, the one named last changes fastest.
Arguments:
- latent: bfloat16 [8192, 4096], P(('sp', 'tp')), may hold values from -6 to 6
- context: bfloat16 [512, 4096], P('sp'), may hold values from -6 to 6
- condition: float32 [4096], replicated, may hold values from -6 to 6
- context_condition: float32 [4096], replicated, may hold values from -6 to 6
- modulation: bfloat16 [3, 4096, 4096], P(None, 'sp', 'tp'), may hold values from -0.09375 to 0.09375
- query_weight: bfloat16 [4096, 4096], P(None, 'tp'), as said below
- key_weight: bfloat16 [4096, 4096], P(None, 'tp'), as said below
- value_weight: bfloat16 [4096, 4096], P(None, 'tp'), may hold values from -0.09375 to 0.09375
- lambdas: float32 [16], P('tp'), may hold values from 0.3 to 0.8
- context_lift: float32 [16], P('tp'), may hold values from 1.5 to 3
- head_gain: float32 [256], replicated, may hold values from 0.1 to 1.9
- output_weight: bfloat16 [4096, 4096], P('tp'), may hold values from -0.09375 to 0.09375
Outputs:
- result: bfloat16 [8192, 4096], P(('sp', 'tp'))
Inputs may be any that keep to these rules, and one draw needn't show every extreme that they name: `query_weight`: entries lie within 200 / sqrt(4096) in magnitude. `key_weight`: entries lie within 6 / sqrt(4096) in magnitude.
All inputs are finite; a program needn't handle non-finite values.
Results may differ from a plain program's by a relative error of at most 0.025.
Values may be sent and summed in bfloat16 or wider, within the bound.
A program may use at most 64 MiB of HBM per device.

v0:
```python
import functools
import math

import jax
import jax.numpy as jnp
from jax import lax
from jax.sharding import Mesh
from jax.sharding import PartitionSpec as P

GRID_W = 64
SP = ("sp_0", "sp_1")
SP_TP = ("sp_0", "sp_1", "tp")


ROPE_BASE = 10000.0
EPSILON = 1e-05


def by_axis(shard, axes):
    return functools.reduce(lax.psum, axes, shard)


def from_everyone(shard, axis):
    copies = jnp.broadcast_to(shard, (lax.axis_size(axis), *shard.shape))
    return lax.all_to_all(copies, axis, split_axis=0, concat_axis=0, tiled=True)


def laid_out(pieces, dim):
    pieces = jnp.moveaxis(pieces, 0, dim)
    lengths = pieces.shape
    return pieces.reshape(*lengths[:dim], lengths[dim] * lengths[dim + 1], *lengths[dim + 2 :])


def collect(shard, axis, dim):
    pieces = from_everyone(shard, axis)
    return laid_out(pieces, dim)


def modulate(tokens_in, offset, scaling):
    values = tokens_in.astype(jnp.float32)
    center = jnp.mean(values, axis=-1, keepdims=True)
    spread = jnp.mean(jnp.square(values - center), axis=-1, keepdims=True)
    normed = (values - center) * lax.rsqrt(spread + EPSILON)
    return (normed * (1.0 + scaling) + offset).astype(jnp.bfloat16)


def rotate(tensor, places):
    number, head_count, head_width = tensor.shape
    quarter = head_width // 4
    eighth = head_width // 8
    inverse = ROPE_BASE ** (-jnp.arange(eighth, dtype=jnp.float32) / eighth)
    grid_row = (places // GRID_W).astype(jnp.float32)
    grid_col = (places % GRID_W).astype(jnp.float32)
    angles = jnp.stack([grid_row[:, None] * inverse, grid_col[:, None] * inverse], axis=1)
    cosine = jnp.cos(angles)[:, None, None, :, :]
    sine_table = jnp.sin(angles)[:, None, None, :, :]
    pieces = tensor.reshape(number, head_count, 2, 2, quarter)
    first_half = pieces[..., :eighth]
    second = pieces[..., eighth:]
    turned = jnp.concatenate(
        [first_half * cosine - second * sine_table, second * cosine + first_half * sine_table],
        axis=-1,
    )
    return turned.reshape(number, head_count, head_width)


def absorb(state_in, key_block, queries, lift_term, scale_factor):
    running_max, running_sum, running_out = state_in
    key_count = key_block.shape[0]
    head_count = queries.shape[1]
    head_width = 2 * queries.shape[3]
    local_width = head_count * head_width
    key_part = key_block[:, :local_width].reshape(key_count, head_count, 2, head_width // 2)
    value_part = key_block[:, local_width:].reshape(key_count, head_count, head_width)
    scores = (
        jnp.einsum("qhmd,khmd->mqhk", queries, key_part, preferred_element_type=jnp.float32)
        * scale_factor
        + lift_term
    )
    new_max = jnp.maximum(running_max, jnp.max(scores, axis=-1))
    fading = jnp.exp(running_max - new_max)
    weights = jnp.exp(scores - new_max[..., None])
    new_sum = running_sum * fading + jnp.sum(weights, axis=-1)
    new_out = running_out * fading[..., None] + jnp.einsum(
        "mqhk,khd->mqhd",
        weights.astype(jnp.bfloat16),
        value_part,
        preferred_element_type=jnp.float32,
    )
    return (new_max, new_sum, new_out)


def shards(
    latent,
    context,
    condition,
    context_condition,
    modulation,
    query_weight,
    key_weight,
    value_weight,
    lambdas,
    context_lift,
    head_gain,
    output_weight,
):
    sp_index = lax.axis_index(SP)
    rows_block = modulation.shape[1]
    silu_pair = jax.nn.silu(jnp.stack([condition, context_condition])).astype(jnp.bfloat16)
    own_rows = lax.dynamic_slice_in_dim(silu_pair, sp_index * rows_block, rows_block, 1)
    partial_mod = jnp.einsum(
        "cd,rde->cre", own_rows, modulation, preferred_element_type=jnp.float32
    )
    summed = by_axis(partial_mod, SP)
    mod_vectors = collect(summed, "tp", 2)
    head_count = lambdas.shape[0]
    head_width = query_weight.shape[1] // head_count
    half_width = head_width // 2
    local_width = head_count * head_width
    scale_factor = half_width ** (-0.5)
    normed = modulate(latent, mod_vectors[0, 0], mod_vectors[0, 1])
    projection = jnp.concatenate([query_weight, key_weight, value_weight], axis=1)
    projected = jnp.dot(
        lax.all_gather(normed, "tp", axis=0, tiled=True),
        projection,
        preferred_element_type=jnp.float32,
    ).astype(jnp.bfloat16)
    block_tokens = projected.shape[0]
    places = sp_index * block_tokens + jnp.arange(block_tokens, dtype=jnp.int32)
    queries = rotate(
        projected[:, :local_width]
        .astype(jnp.float32)
        .reshape(block_tokens, head_count, head_width),
        places,
    )
    queries = queries.astype(jnp.bfloat16).reshape(block_tokens, head_count, 2, half_width)
    latent_keys = rotate(
        projected[:, local_width : 2 * local_width]
        .astype(jnp.float32)
        .reshape(block_tokens, head_count, head_width),
        places,
    )
    latent_keys = latent_keys.astype(jnp.bfloat16).reshape(block_tokens, local_width)
    packed = jnp.concatenate([latent_keys, projected[:, 2 * local_width :]], axis=1)
    normed_context = modulate(context, mod_vectors[1, 0], mod_vectors[1, 1])
    own_context = jnp.dot(
        normed_context, projection[:, local_width:], preferred_element_type=jnp.float32
    ).astype(jnp.bfloat16)
    context_packed = collect(own_context, SP, 0)
    initial = (
        jnp.full((2, block_tokens, head_count), -jnp.inf, jnp.float32),
        jnp.zeros((2, block_tokens, head_count), jnp.float32),
        jnp.zeros((2, block_tokens, head_count, head_width), jnp.float32),
    )
    state_now = absorb(initial, context_packed, queries, context_lift[:, None], scale_factor)
    segment = lax.all_gather(packed, SP, axis=0, tiled=True)
    length = segment.shape[0]
    block_len = math.gcd(length, 1024)
    stacked = segment.reshape(length // block_len, block_len, segment.shape[1])

    def one_block(state_step, block_rows):
        return (absorb(state_step, block_rows, queries, 0.0, scale_factor), None)

    running_max, running_sum, running_out = lax.scan(one_block, state_now, stacked)[0]
    means = running_out / running_sum[..., None]
    difference = means[0] - lambdas[None, :, None] * means[1]
    scaled = (
        difference
        * lax.rsqrt(jnp.mean(jnp.square(difference), axis=-1, keepdims=True) + EPSILON)
        * head_gain
    )
    attended = scaled.astype(jnp.bfloat16).reshape(block_tokens, local_width)
    mixture = lax.psum_scatter(
        jnp.dot(attended, output_weight, preferred_element_type=jnp.float32).astype(jnp.bfloat16),
        "tp",
        scatter_dimension=0,
        tiled=True,
    ).astype(jnp.float32)
    return (latent.astype(jnp.float32) + mod_vectors[0, 2] * mixture).astype(jnp.bfloat16)


def solution(mesh):
    split = Mesh(mesh.devices.reshape(4, 4, mesh.shape["tp"]), ("sp_0", "sp_1", "tp"))
    return jax.shard_map(
        shards,
        mesh=split,
        in_specs=(
            P(SP_TP, None),
            P(SP, None),
            P(),
            P(),
            P(None, SP, "tp"),
            P(None, "tp"),
            P(None, "tp"),
            P(None, "tp"),
            P("tp"),
            P("tp"),
            P(),
            P("tp", None),
        ),
        out_specs=P(SP_TP, None),
        check_vma=False,
    )
```

profile of v0, /device:TPU:1, one launch (start us, length us, event | category | flops | bytes accessed | tf_op | source)
XLA Modules:
  0.0 302.9 jit_solution(5398257934742290326)
XLA Ops:
  6.5 1.4 fusion.78
  7.9 9.6 %psum.14 = f32[2,3,256]{2,0,1:T(2,128)S(1)} all-reduce(f32[2,3,256]{2,0,1:T(2,128)S(1)} %fusion.78), channel_id=1, replica_groups=mesh['sp_0'=4,'sp_1'=4,'tp'=16] {'sp_0'}, use_global_device_ids=true, to_apply=%region_0.1 | all-reduce | flops 1536 | bytes 12288 | tf_op jit(solution)/shard_map/psum | solution.py:20
  17.6 8.9 %psum.15 = f32[2,3,256]{2,0,1:T(2,128)S(1)} all-reduce(f32[2,3,256]{2,0,1:T(2,128)S(1)} %psum.14), channel_id=1, replica_groups=mesh['sp_0'=4,'sp_1'=4,'tp'=16] {'sp_1'}, use_global_device_ids=true, to_apply=%region_1.2 | all-reduce | flops 1536 | bytes 12288 | tf_op jit(solution)/shard_map/psum | solution.py:20
  27.2 12.8 %all-to-all-start = ((f32[16,2,3,256]{3,1,2,0:T(2,128)}), f32[16,2,3,256]{3,1,2,0:T(2,128)S(1)}, u32[]{:S(2)}, u32[]{:S(2)}) async-start(f32[16,2,3,256]{3,1,2,0:T(2,128)} %broadcast_in_dim.12), calls=%async_computation | async-start | bytes 196608 | tf_op jit(solution)/shard_map/all_to_all | solution.py:25
  42.4 6.1 %all-to-all-done = f32[16,2,3,256]{3,1,2,0:T(2,128)S(1)} async-done(((f32[16,2,3,256]{3,1,2,0:T(2,128)}), f32[16,2,3,256]{3,1,2,0:T(2,128)S(1)}, u32[]{:S(2)}, u32[]{:S(2)}) %all-to-all-start) | async-done | bytes 98336 | tf_op jit(solution)/shard_map/all_to_all | solution.py:25
  48.6 1.8 fusion.51
  51.0 33.7 %all-gather.3.cloned.1.call-done = bf16[512,4096]{1,0:T(8,128)(2,1)} async-done(((bf16[32,4096]{1,0:T(8,128)(2,1)}), bf16[512,4096]{1,0:T(8,128)(2,1)}) %all-gather.3.cloned.1.call-update) | async-done | bytes 4194320 | tf_op jit(solution)/shard_map/all_gather | solution.py:124
  84.8 7.5 %fusion.31 = bf16[512,768]{1,0:T(8,128)(2,1)S(1)} fusion(bf16[512,4096]{1,0:T(8,128)(2,1)} %all-gather.3.cloned.1.call-done, bf16[4096,256]{1,0:T(8,128)(2,1)} %param.21, bf16[4096,256]{1,0:T(8,128)(2,1)} %param.20, bf16[4096,256]{1,0:T(8,128)(2,1)} %param.19), kind=kOutput, calls=%fused_computation.37 | convolution fusion | flops 3240493056 | bytes 11272192 | tf_op jit(solution)/shard_map/dot_general | solution.py:123
  94.7 1.8 pad_maximum_fusion
  98.8 3.2 %fusion.36 = bf16[32,512]{1,0:T(8,128)(2,1)S(1)} fusion(bf16[4096,256]{1,0:T(8,128)(2,1)} %param.21, bf16[4096,256]{1,0:T(8,128)(2,1)} %param.20, bf16[32,4096]{1,0:T(8,128)(2,1)} %param.15, f32[4096]{0:T(1024)S(1)} %bitcast.171, f32[4096]{0:T(1024)S(1)} %bitcast.172, f32[32]{0:T(128)S(1)} %add_rsqrt_fusion.2, f32[32]{0:T(128)S(1)} %broadcast_multiply_fusion.3), kind=kOutput, calls=%fused_computation.41 | convolution fusion | flops 143409152 | bytes 4522240 | tf_op jit(solution)/shard_map/dot_general | solution.py:146
  102.9 6.5 %all-to-all-start.1 = ((bf16[16,32,512]{2,1,0:T(8,128)(2,1)}), bf16[16,32,512]{2,1,0:T(8,128)(2,1)S(1)}, u32[]{:S(2)}, u32[]{:S(2)}) async-start(bf16[16,32,512]{2,1,0:T(8,128)(2,1)} %broadcast_in_dim.13), calls=%async_computation.1 | async-start | bytes 1048576 | tf_op jit(solution)/shard_map/all_to_all | solution.py:25
  111.0 15.4 %all-to-all-done.1 = bf16[16,32,512]{2,1,0:T(8,128)(2,1)S(1)} async-done(((bf16[16,32,512]{2,1,0:T(8,128)(2,1)}), bf16[16,32,512]{2,1,0:T(8,128)(2,1)S(1)}, u32[]{:S(2)}, u32[]{:S(2)}) %all-to-all-start.1) | async-done | bytes 524320 | tf_op jit(solution)/shard_map/all_to_all | solution.py:25
  127.2 1.8 copy.35
  129.5 1.5 bitcast_reduce_fusion.1
  131.5 1.7 fusion.35
  133.2 41.4 %all-gather.5.cloned.1.call-done = bf16[8192,512]{1,0:T(8,128)(2,1)} async-done(((bf16[512,512]{1,0:T(8,128)(2,1)}), bf16[8192,512]{1,0:T(8,128)(2,1)}) %all-gather.5.cloned.1.call-update) | async-done | bytes 8388624 | tf_op jit(solution)/shard_map/all_gather | solution.py:156
  174.6 54.9 %while.14 = (s32[]{:T(128)}, f32[2,512,1]{1,0,2:T(2,128)S(1)}, f32[2,512,1]{1,0,2:T(2,128)S(1)}, f32[2,512,1,256]{1,3,0,2:T(8,128)}, bf16[8,1024,512]{2,1,0:T(8,...) while((s32[]{:T(128)}, f32[2,512,1]{1,0,2:T(2,128)S(1)}, f32[2,512,1]{1,0,2:T(2,128)S(1)}, ...), condition=%wide.region_11.12_spmd, body=%wide.region_8.11_spmd.sunk | while | flops 814222336 | bytes 33882276 | solution.py:164
  174.6 1.3 constant_dynamic-slice_fusion.2
  175.9 1.3 copy.54
  181.5 1.3 constant_dynamic-slice_fusion.2
  182.8 1.3 copy.54
  188.4 1.3 constant_dynamic-slice_fusion.2
  189.7 1.3 copy.54
  196.5 1.3 copy.54
  203.4 1.3 copy.54
  210.3 1.3 copy.54
  217.1 1.3 copy.54
  224.0 1.3 copy.54
  229.5 1.4 broadcast_divide_fusion
  231.1 3.3 %convolution_convert_fusion = bf16[512,4096]{1,0:T(8,128)(2,1)} fusion(bf16[256,4096]{1,0:T(8,128)(2,1)S(1)} %copy-done, f32[256]{0:T(256)S(1)} %copy-done.7, f32[512]{0:T(512)S(1)} %add_rsqrt_fusion, f32[2,512,1,256]{1,3,0,2:T(8,128)S(1)} %broadcast_divide_fusion, f32[]{:T(128)} %bitcast.145), kind=kOutput, calls=%fused_computation.26 | convolution fusion | flops 1076494336 | bytes 7343108 | tf_op jit(solution)/shard_map/dot_general | solution.py:174
  234.4 60.2 %reduce-scatter.2.cloned.1.call-done = bf16[32,4096]{1,0:T(8,128)(2,1)} async-done(((bf16[512,4096]{1,0:T(8,128)(2,1)}), bf16[32,4096]{1,0:T(8,128)(2,1)}) %reduce-scatter.2.cloned.1.call-update) | async-done | bytes 262160 | tf_op jit(solution)/shard_map/reduce_scatter | solution.py:173
  294.7 1.7 fusion.56
  (156 shorter events, 51.5 us)
Async XLA Ops:
  6.5 224.5 %copy-start = (bf16[256,4096]{1,0:T(8,128)(2,1)S(1)}, bf16[256,4096]{1,0:T(8,128)(2,1)}, u32[]{:S(2)}) copy-start(bf16[256,4096]{1,0:T(8,128)(2,1)} %param.25) | copy-start | bytes 6291460
  27.2 21.3 %all-to-all-start = ((f32[16,2,3,256]{3,1,2,0:T(2,128)}), f32[16,2,3,256]{3,1,2,0:T(2,128)S(1)}, u32[]{:S(2)}, u32[]{:S(2)}) async-start(f32[16,2,3,256]{3,1,2,0:T(2,128)} %broadcast_in_dim.12), calls=%async_computation | async-start | bytes 196608 | tf_op jit(solution)/shard_map/all_to_all | solution.py:25
  40.0 44.7 %all-gather.3.cloned.1.call-start = ((), (), s32[]{:S(2)}) async-start(), calls=%async_computation.3 | async-start | bytes 4456448 | tf_op jit(solution)/shard_map/all_gather | solution.py:124
  50.4 124.2 %all-gather.5.cloned.1.call-start = ((), (), s32[]{:S(2)}) async-start(), calls=%async_computation.4 | async-start | bytes 8912896 | tf_op jit(solution)/shard_map/all_gather | solution.py:156
  102.9 23.5 %all-to-all-start.1 = ((bf16[16,32,512]{2,1,0:T(8,128)(2,1)}), bf16[16,32,512]{2,1,0:T(8,128)(2,1)S(1)}, u32[]{:S(2)}, u32[]{:S(2)}) async-start(bf16[16,32,512]{2,1,0:T(8,128)(2,1)} %broadcast_in_dim.13), calls=%async_computation.1 | async-start | bytes 1048576 | tf_op jit(solution)/shard_map/all_to_all | solution.py:25
  109.5 185.2 %reduce-scatter.2.cloned.1.call-start = ((), (), s32[]{:S(2)}) async-start(), calls=%async_computation.5 | async-start | bytes 4456448 | tf_op jit(solution)/shard_map/reduce_scatter | solution.py:173
  126.4 2.6 copy-start.5
  129.3 2.1 copy-start.6
  174.6 56.4 %copy-start.7 = (f32[256]{0:T(256)S(1)}, f32[256]{0:T(256)}, u32[]{:S(2)}) copy-start(f32[256]{0:T(256)} %param.24) | copy-start | bytes 3076
  177.3 2.0 copy-start.1
  177.3 2.0 copy-start.2
  180.4 1.1 copy-start.3
  184.1 2.0 copy-start.1
  184.1 2.0 copy-start.2
  187.3 1.1 copy-start.3
  191.0 2.0 copy-start.1
  191.0 2.0 copy-start.2
  194.2 1.1 copy-start.3
  197.8 2.0 copy-start.1
  197.8 2.0 copy-start.2
  201.0 1.1 copy-start.3
  204.7 2.0 copy-start.1
  204.7 2.0 copy-start.2
  207.9 1.1 copy-start.3
  211.6 2.0 copy-start.1
  211.6 2.0 copy-start.2
  214.8 1.1 copy-start.3
  218.4 2.0 copy-start.1
  218.4 2.0 copy-start.2
  225.3 2.0 copy-start.1
  225.3 2.0 copy-start.2
  231.1 63.6 %copy-start.4 = (bf16[32,4096]{1,0:T(8,128)(2,1)S(1)}, bf16[32,4096]{1,0:T(8,128)(2,1)}, u32[]{:S(2)}) copy-start(bf16[32,4096]{1,0:T(8,128)(2,1)} %param.14) | copy-start | bytes 786436
  (2 other events, 2.1 us)
Sparse Core Ops, SparseCore 0:
  50.5 34.1 all-gather.2
  96.6 77.9 all-gather.4
  234.5 60.0 reduce-scatter.1
where the time goes:
time: 306 us; the launch traced here: 303 us
  waiting for transfers between devices  157 us (51%)
  local copies, waits for them, and re-layouts  39.2 us (13%)
  matrix products  33.8 us (11%)
  starting transfers between devices  19.7 us (6%)
  other arithmetic  19.6 us (6%)
  blocking collectives  18.6 us (6%)
  between operations  14.6 us (5%)
    reduce_scatter x1, waiting for transfers between devices, shards(): lax.psum_scatter(jnp.dot(attended, output_weight, preferred_element_type=...  60.2 us
    all_gather x1, waiting for transfers between devices, shards(): segment = lax.all_gather(packed, SP, axis=0, tiled=True)  41.4 us
    all_gather x1, waiting for transfers between devices, shards(): lax.all_gather(normed, 'tp', axis=0, tiled=True)  33.7 us
    all_to_all x2, waiting for transfers between devices, from_everyone(): return lax.all_to_all(copies, axis, split_axis=0, concat_axis=0, tiled=True)  21.5 us
    dynamic_slice x16, local copies, waits for them, and re-layouts, shards(): lax.scan(one_block, state_now, stacked)[0]  20.8 us
    all_to_all x2, starting transfers between devices, from_everyone(): return lax.all_to_all(copies, axis, split_axis=0, concat_axis=0, tiled=True)  19.4 us
    psum x2, blocking collectives, by_axis(): return functools.reduce(lax.psum, axes, shard)  18.6 us
    slice x10, local copies, waits for them, and re-layouts, absorb(): key_block[:, :local_width]  12.4 us
  transfers between devices with their start and end apart: 5, of which 5 were waited for; matrix products, arithmetic and copies ran while one was open for 5% of the time, Pallas kernels for 0%

commit v1 on v0

v1 whole, which is shorter than its diff:
```python
import functools
import math

import jax
import jax.numpy as jnp
import numpy as np
from jax import lax
from jax.experimental import pallas as pl
from jax.experimental.pallas import tpu as pltpu
from jax.sharding import Mesh
from jax.sharding import PartitionSpec as P

MESH = pl.DeviceIdType.MESH
F32 = jnp.float32
BF16 = jnp.bfloat16
GRID_W = 64
EPS = 1e-5
NZ = 8
NS = 16
D = 4096
HD = 256
PART = 128
ROWS = 32
LOG2E = math.log2(math.e)
ORDER = (0, 7, 1, 6, 2, 5, 3, 4)
PLACE = {rel: i for i, rel in enumerate(ORDER)}
UNIT = 2 * ROWS
BLOCK = NZ * UNIT
ANY = pl.BlockSpec(memory_space=pl.ANY)
VM = pl.BlockSpec(memory_space=pltpu.VMEM)
SM = pl.BlockSpec(memory_space=pltpu.SMEM)


def position():
    return tuple(lax.axis_index(a) for a in ("y", "x", "z", "c"))


def sp_peer(i):
    y, x, z, c = position()
    peer = lax.rem(y * 4 + x + i, NS)
    return (peer // 4, lax.rem(peer, 4), z, c)


def tp_peer(i):
    y, x, z, c = position()
    peer = lax.rem(z * 2 + c + i, NS)
    return (y, x, peer // 2, lax.rem(peer, 2))


def greet(peers):
    barrier = pltpu.get_barrier_semaphore()
    for peer_of in peers:

        def one(i, carry):
            pl.semaphore_signal(barrier, inc=1, device_id=peer_of(i), device_id_type=MESH)
            return carry

        lax.fori_loop(1, NS, one, 0)


def greeted(peers):
    pl.semaphore_wait(pltpu.get_barrier_semaphore(), (NS - 1) * len(peers))


def send(src, dst, send_sem, recv_sem, to):
    pltpu.make_async_remote_copy(
        src_ref=src, dst_ref=dst, send_sem=send_sem, recv_sem=recv_sem, device_id=to, device_id_type=MESH
    ).start()


def await_bytes(ref, sem):
    pltpu.make_async_copy(ref, ref, sem).wait()


def silu(v):
    return v / (1.0 + jnp.exp(-v))


def modulated(tokens, shift, scale):
    values = tokens.astype(F32)
    center = jnp.mean(values, axis=-1, keepdims=True)
    values = values - center
    spread = jnp.mean(values * values, axis=-1, keepdims=True)
    return (values * lax.rsqrt(spread + EPS) * (1.0 + scale) + shift).astype(BF16)


def turned(raw, cos, sin):
    lane = lax.broadcasted_iota(jnp.int32, raw.shape, 1)
    partner = jnp.where(lax.rem(lane, 64) < 32, pltpu.roll(raw, HD - 32, 1), pltpu.roll(raw, 32, 1))
    return (raw * cos + partner * sin).astype(BF16)


def tables():
    inverse = 10000.0 ** (-np.arange(32, dtype=np.float32) / np.float32(32))
    inverse = inverse.astype(np.float32)
    row = (np.arange(128, dtype=np.float32)[:, None] * inverse).astype(np.float32).astype(np.float64)
    col = row[:GRID_W]
    zr, zc = np.zeros((128, 64)), np.zeros((GRID_W, 64))

    def lanes(first, second):
        return np.tile(np.concatenate([first, second], axis=1), (1, 2)).astype(np.float32)

    both = lambda a, b: np.concatenate([a, b], axis=1)
    return (
        lanes(both(np.cos(row), np.cos(row)), zr),
        lanes(both(-np.sin(row), np.sin(row)), zr),
        lanes(zc, both(np.cos(col), np.cos(col))),
        lanes(zc, both(-np.sin(col), np.sin(col))),
    )


def front(
    latent, context, cond, ctx_cond, modulation, wq, wk, wv, rcos, rsin, ccos, csin,
    q_out, kv_out, ctx_out, mods,
    lat, wq_v, wk_v, wv_v, mod_v, ctx_v, parts, normed,
    load, mod_send, mod_recv, ring_send, ring_recv, pair_send, pair_recv,
):
    y, x, z, c = position()
    sp, tp = y * 4 + x, z * 2 + c
    loads = [
        pltpu.make_async_copy(latent, lat.at[z, c], load.at[0]),
        pltpu.make_async_copy(modulation, mod_v, load.at[1]),
        pltpu.make_async_copy(context, ctx_v, load.at[2]),
        pltpu.make_async_copy(wq, wq_v, load.at[3]),
        pltpu.make_async_copy(wk, wk_v, load.at[4]),
        pltpu.make_async_copy(wv, wv_v, load.at[5]),
    ]
    for copy in loads:
        copy.start()

    def half_of(step, way):
        return (0, 1) if step < 4 else ((0,) if way > 0 else (1,))

    def block(rel):
        return lax.rem(z + rel, NZ)

    def ring_step(step, way, half):
        held = block((-way * (step - 1)) % NZ)
        there = (-way * step) % NZ
        rows = pl.ds(half * 16, 16)
        send(
            lat.at[held, c, rows], lat.at[held, c, rows], ring_send.at[there * 2 + half],
            ring_recv.at[there * 2 + half], (y, x, lax.rem(z + way + NZ, NZ), c),
        )

    def ring_wait(rel, half):
        await_bytes(lat.at[block(rel), c, pl.ds(half * 16, 16)], ring_recv.at[rel * 2 + half])

    def pair_step(rel):
        mine = lat.at[block(rel), c]
        send(mine, mine, pair_send.at[rel], pair_recv.at[rel], (y, x, z, 1 - c))

    def pair_wait(rel):
        await_bytes(lat.at[block(rel), 1 - c], pair_recv.at[rel])

    loads[0].wait()
    greeted((sp_peer, tp_peer))
    for half in (0, 1):
        for way in (1, -1):
            ring_step(1, way, half)
    pair_step(0)

    pick = lax.broadcasted_iota(jnp.int32, (8, PART), 0) == 0
    rows = []
    for j in range(2):
        at = pl.ds(sp * 2 + j, 1)
        rows.append(silu(jnp.where(pick, cond[at, :], ctx_cond[at, :])).astype(BF16))
    loads[1].wait()
    for r in range(3):
        product = jnp.dot(rows[0], mod_v[r, 0:PART], preferred_element_type=F32) + jnp.dot(
            rows[1], mod_v[r, PART : 2 * PART], preferred_element_type=F32
        )
        parts[sp, r : r + 1, :] = product[0:1]
        parts[sp, 3 + r : 4 + r, :] = product[1:2]
    parts[sp, 6:8, :] = jnp.zeros((2, HD), F32)

    def show_part(i, carry):
        send(parts.at[sp], parts.at[sp], mod_send.at[0], mod_recv.at[0], sp_peer(i))
        return carry

    lax.fori_loop(1, NS, show_part, 0)
    await_bytes(parts.at[pl.ds(0, NS - 1)], mod_recv.at[0])
    total = parts[0]
    for i in range(1, NS):
        total = total + parts[i]
    own_cols = pl.ds(pl.multiple_of(tp * HD, HD), HD)
    mods[:, own_cols] = total

    def show_sum(i, carry):
        send(mods.at[:, own_cols], mods.at[:, own_cols], mod_send.at[1], mod_recv.at[1], tp_peer(i))
        return carry

    lax.fori_loop(1, NS, show_sum, 0)

    def forward(step):
        for half in (0, 1):
            for way in (1, -1):
                ring_wait((-way * step) % NZ, half)
                if half in half_of(step + 1, way):
                    ring_step(step + 1, way, half)
        for way in (1, -1):
            pair_step((-way * step) % NZ)

    def norm_rows(load_rows, where, pick_mod):
        shift, scale = mods[pick_mod : pick_mod + 1, :], mods[pick_mod + 1 : pick_mod + 2, :]
        for half in (0, 1):
            normed[where + half * 16 : where + half * 16 + 16, :] = modulated(
                load_rows(pl.ds(half * 16, 16)), shift, scale
            )

    def project(units, with_context):
        count = len(units)
        for i, rel in enumerate(units):
            zz = block(rel)
            for core in (0, 1):
                norm_rows(lambda rows, zz=zz, core=core: lat[zz, core, rows, :], i * UNIT + core * ROWS, 0)
        if with_context:
            norm_rows(lambda rows: ctx_v[rows, :], count * UNIT, 3)
        end = count * UNIT + (ROWS if with_context else 0)
        lhs = normed[0:end, :]
        q_raw = jnp.dot(lhs, wq_v[...], preferred_element_type=F32).astype(BF16)
        k_raw = jnp.dot(lhs, wk_v[...], preferred_element_type=F32).astype(BF16)
        v_raw = jnp.dot(lhs, wv_v[...], preferred_element_type=F32).astype(BF16)
        for i, rel in enumerate(units):
            o = PLACE[rel]
            line = pl.ds(sp * NZ + block(rel), 1)
            cos = rcos[line, :] + ccos[...]
            sin = rsin[line, :] + csin[...]
            part = slice(i * UNIT, (i + 1) * UNIT)
            q = turned(q_raw[part].astype(F32), cos, sin)
            for core in (0, 1):
                q_out[core * HD + o * ROWS : core * HD + (o + 1) * ROWS, :] = q[core * ROWS : (core + 1) * ROWS]
            kv_out[o, :, 0:HD] = turned(k_raw[part].astype(F32), cos, sin)
            kv_out[o, :, HD : 2 * HD] = v_raw[part]
        if with_context:
            ctx_out[:, 0:HD] = k_raw[count * UNIT : end]
            ctx_out[:, HD : 2 * HD] = v_raw[count * UNIT : end]

    forward(1)
    await_bytes(mods.at[:, pl.ds(0, (NS - 1) * HD)], mod_recv.at[1])
    for copy in loads[2:]:
        copy.wait()
    pair_wait(0)
    project([0], True)
    forward(2)
    for rel in (7, 1):
        pair_wait(rel)
    project([7, 1], False)
    forward(3)
    for rel in (6, 2):
        pair_wait(rel)
    project([6, 2], False)
    ring_wait(4, 0)
    ring_wait(4, 1)
    pair_step(4)
    for rel in (5, 3):
        pair_wait(rel)
    project([5, 3], False)
    pair_wait(4)
    project([4], False)

    await_bytes(parts.at[pl.ds(0, NS - 1)], mod_send.at[0])
    await_bytes(mods.at[:, pl.ds(0, (NS - 1) * HD)], mod_send.at[1])
    for i in range(2, 2 * NZ):
        await_bytes(lat.at[0, 0, pl.ds(0, 16)], ring_send.at[i])
    for rel in range(NZ):
        await_bytes(lat.at[0, 0], pair_send.at[rel])


def front_kernel(*refs):
    greet((sp_peer, tp_peer))
    front(*refs)


def run_front(latent, context, cond, ctx_cond, modulation, wq, wk, wv):
    dma = pltpu.SemaphoreType.DMA
    return pl.pallas_call(
        front_kernel,
        out_shape=(
            jax.ShapeDtypeStruct((BLOCK, HD), BF16),
            jax.ShapeDtypeStruct((NZ, UNIT, 2 * HD), BF16),
            jax.ShapeDtypeStruct((ROWS, 2 * HD), BF16),
            jax.ShapeDtypeStruct((8, D), F32),
        ),
        in_specs=[ANY, ANY, VM, VM, ANY, ANY, ANY, ANY, VM, VM, VM, VM],
        out_specs=(VM, VM, VM, VM),
        scratch_shapes=[
            pltpu.VMEM((NZ, 2, ROWS, D), BF16),
            pltpu.VMEM((D, HD), BF16),
            pltpu.VMEM((D, HD), BF16),
            pltpu.VMEM((D, HD), BF16),
            pltpu.VMEM((3, HD, HD), BF16),
            pltpu.VMEM((ROWS, D), BF16),
            pltpu.VMEM((NS, 8, HD), F32),
            pltpu.VMEM((2 * UNIT, D), BF16),
            dma((6,)),
            dma((2,)),
            dma((2,)),
            dma((2 * NZ,)),
            dma((2 * NZ,)),
            dma((NZ,)),
            dma((NZ,)),
        ],
        compiler_params=pltpu.CompilerParams(
            collective_id=0, has_side_effects=True, vmem_limit_bytes=40 * 2**20
        ),
        name="front",
    )(latent, context, cond, ctx_cond, modulation, wq, wk, wv, *[jnp.asarray(t) for t in tables()])


def gather_unit(kv, kv_send, kv_recv):
    y, x, z, c = position()

    def geometry(o):
        swap = lax.rem(o, 2)
        way = 1 - 2 * lax.rem(o // 2, 2)
        first = swap * y + (1 - swap) * x
        second = swap * x + (1 - swap) * y
        return swap, way, first, second

    def step(o, geo, df, dg, tf, tg, kind):
        swap, way, first, second = geo

        def pair(f, g):
            f, g = lax.rem(f + 8, 4), lax.rem(g + 8, 4)
            return swap * f + (1 - swap) * g, swap * g + (1 - swap) * f

        oy, ox = pair(first + df, second + dg)
        ty, tx = pair(first + tf, second + tg)
        rows = pl.ds(pl.multiple_of((oy * 4 + ox) * UNIT, UNIT), UNIT)
        send(kv.at[o, rows], kv.at[o, rows], kv_send.at[0], kv_recv.at[o * 5 + kind], (ty, tx, z, c))

    def wait(o, kind, count):
        await_bytes(kv.at[o, pl.ds(0, count * UNIT)], kv_recv.at[o * 5 + kind])

    def own(o):
        geo = geometry(o)
        way = geo[1]
        step(o, geo, 0, 0, 1, 0, 0)
        step(o, geo, 0, 0, -1, 0, 0)
        step(o, geo, 0, 0, 0, way, 1)
        step(o, geo, 0, 0, 0, -way, 4)

    def stage1(o):
        geo = geometry(o)
        way = geo[1]
        wait(o, 0, 2)
        step(o, geo, -way, 0, way, 0, 1)
        for d in (1, -1):
            step(o, geo, d, 0, 0, way, 2)
            step(o, geo, d, 0, 0, -way, 4)

    def stage2(o):
        geo = geometry(o)
        way = geo[1]
        wait(o, 1, 2)
        step(o, geo, 2, 0, 0, way, 3)
        step(o, geo, 2, 0, 0, -way, 4)
        step(o, geo, 0, -way, 0, way, 4)

    def stage3(o):
        geo = geometry(o)
        way = geo[1]
        wait(o, 2, 2)
        for d in (1, -1):
            step(o, geo, d, -way, 0, way, 4)

    def stage4(o):
        geo = geometry(o)
        way = geo[1]
        wait(o, 3, 1)
        step(o, geo, 2, -way, 0, way, 4)

    def done(o):
        wait(o, 4, 8)

    def all_sent():
        for _ in range(NS - 1):
            await_bytes(kv.at[0, pl.ds(0, NZ * UNIT)], kv_send.at[0])

    return own, (stage1, stage2, stage3, stage4), done, all_sent


def absorb(q, key_part, value_part, lift, peak, sums, acc):
    factor = PART**-0.5 * LOG2E
    values = value_part()
    for m in range(2):
        scores = lax.dot_general(
            q[:, m * PART : (m + 1) * PART], key_part(m), (((1,), (1,)), ((), ())), preferred_element_type=F32
        )
        scores = scores * factor
        if lift is not None:
            scores = scores + lift
        before = peak[m]
        now = jnp.maximum(before, jnp.max(scores, axis=1, keepdims=True))
        fading = jnp.exp2(before - now)
        weights = jnp.exp2(scores - now[:, 0:1])
        sums[m] = sums[m] * fading + jnp.sum(weights, axis=1, keepdims=True)
        acc[m] = acc[m] * fading[:, 0:1] + jnp.dot(
            weights.astype(BF16), values, preferred_element_type=F32
        )
        peak[m] = now


def middle(
    q, kv_own, ctx_own, lift, lam, gain,
    attended,
    kv, ctx, peak, sums, acc,
    load, ctx_send, ctx_recv, kv_send, kv_recv,
):
    y, x, z, c = position()
    sp = y * 4 + x
    loads = [
        pltpu.make_async_copy(kv_own, kv.at[:, pl.ds(pl.multiple_of(sp * UNIT, UNIT), UNIT)], load.at[0]),
        pltpu.make_async_copy(ctx_own, ctx.at[pl.ds(pl.multiple_of(sp * ROWS, ROWS), ROWS)], load.at[1]),
    ]
    for copy in loads:
        copy.start()
    peak[...] = jnp.full(peak.shape, -jnp.inf, F32)
    sums[...] = jnp.zeros(sums.shape, F32)
    acc[...] = jnp.zeros(acc.shape, F32)
    own, stages, done, all_sent = gather_unit(kv, kv_send, kv_recv)
    for copy in loads:
        copy.wait()
    greeted((sp_peer,))

    def show_context(i, carry):
        mine = ctx.at[pl.ds(pl.multiple_of(sp * ROWS, ROWS), ROWS)]
        send(mine, mine, ctx_send.at[0], ctx_recv.at[0], sp_peer(i))
        return carry

    lax.fori_loop(1, NS, show_context, 0)

    def start_own(o, carry):
        own(o)
        return carry

    lax.fori_loop(0, NZ, start_own, 0)
    lift_term = lift[0] * LOG2E

    def tick(t, carry):
        for back, stage in enumerate(stages):
            o = t - back

            @pl.when((o >= 0) & (o < NZ))
            def _():
                stage(o)

        @pl.when(t == 1)
        def _():
            await_bytes(ctx.at[pl.ds(0, (NS - 1) * ROWS)], ctx_recv.at[0])
            absorb(
                q, lambda m: ctx[:, m * PART : (m + 1) * PART], lambda: ctx[:, HD : 2 * HD],
                lift_term, peak, sums, acc,
            )

        o = t - len(stages)

        @pl.when(o >= 0)
        def _():
            done(o)

            def part(i, inner):
                rows = pl.ds(pl.multiple_of(i * 512, 512), 512)
                absorb(
                    q, lambda m: kv[o, rows, m * PART : (m + 1) * PART], lambda: kv[o, rows, HD : 2 * HD],
                    None, peak, sums, acc,
                )
                return inner

            lax.fori_loop(0, 2, part, 0)

        return carry

    lax.fori_loop(0, NZ + len(stages), tick, 0)
    means = [acc[m] / sums[m][:, 0:1] for m in range(2)]
    difference = means[0] - lam[0] * means[1]
    spread = jnp.mean(difference * difference, axis=1, keepdims=True)
    attended[...] = (difference * lax.rsqrt(spread + EPS) * gain[...]).astype(BF16)
    all_sent()
    await_bytes(ctx.at[pl.ds(0, (NS - 1) * ROWS)], ctx_send.at[0])


def middle_kernel(*refs):
    greet((sp_peer,))
    middle(*refs)


def run_middle(q, kv_own, ctx_own, lift, lam, gain):
    dma = pltpu.SemaphoreType.DMA
    return pl.pallas_call(
        middle_kernel,
        out_shape=jax.ShapeDtypeStruct((BLOCK, HD), BF16),
        in_specs=[VM, ANY, ANY, SM, SM, VM],
        out_specs=VM,
        scratch_shapes=[
            pltpu.VMEM((NZ, NS * UNIT, 2 * HD), BF16),
            pltpu.VMEM((NS * ROWS, 2 * HD), BF16),
            pltpu.VMEM((2, BLOCK, 128), F32),
            pltpu.VMEM((2, BLOCK, 128), F32),
            pltpu.VMEM((2, BLOCK, HD), F32),
            dma((2,)),
            dma((1,)),
            dma((1,)),
            dma((1,)),
            dma((5 * NZ,)),
        ],
        compiler_params=pltpu.CompilerParams(
            collective_id=1, has_side_effects=True, vmem_limit_bytes=40 * 2**20
        ),
        name="middle",
    )(q, kv_own, ctx_own, lift, lam, gain)


CHUNKS = 4
WIDE = D // CHUNKS


def back(
    attended, wo, latent, mods,
    result,
    mine, theirs, wo_v, wo_pair, lat_v, part, out_buf, in_buf,
    load, pair_send, pair_recv, out_send, out_recv,
):
    y, x, z, c = position()
    pair = (y, x, z, 1 - c)
    loads = [
        pltpu.make_async_copy(wo, wo_v, load.at[0]),
        pltpu.make_async_copy(attended.at[pl.ds(pl.multiple_of(c * HD, HD), HD)], mine, load.at[1]),
        pltpu.make_async_copy(latent, lat_v, load.at[2]),
    ]
    for copy in loads:
        copy.start()
    greeted((tp_peer,))
    send(attended.at[pl.ds(pl.multiple_of((1 - c) * HD, HD), HD)], theirs, pair_send.at[0], pair_recv.at[0], pair)
    loads[0].wait()
    send(wo_v, wo_pair, pair_send.at[1], pair_recv.at[1], pair)
    loads[1].wait()
    await_bytes(theirs, pair_recv.at[0])
    await_bytes(wo_pair, pair_recv.at[1])

    def long_way(j):
        return 0 if j < 2 else 1

    def slot(way, step, j):
        return (way * 4 + step - 1) * CHUNKS + j

    def hop(way, step, j, add):
        rel = (5 - step) if way == 0 else (3 + step) % NZ
        value = part[j, PLACE[rel]]
        if add:
            value = value + in_buf[slot(way, step - 1, j)].astype(F32)
        s = slot(way, step, j)
        out_buf[s] = value.astype(BF16)
        to = lax.rem(z + (1 if way == 0 else NZ - 1), NZ)
        send(out_buf.at[s], in_buf.at[s], out_send.at[s], out_recv.at[s], (y, x, to, c))

    def hop_wait(way, step, j):
        s = slot(way, step, j)
        await_bytes(in_buf.at[s], out_recv.at[s])

    for j in (0, 2, 1, 3):
        cols = slice(j * WIDE, (j + 1) * WIDE)
        product = jnp.dot(mine[...], wo_v[:, cols], preferred_element_type=F32) + jnp.dot(
            theirs[...], wo_pair[:, cols], preferred_element_type=F32
        )
        part[j] = product.reshape(NZ, ROWS, WIDE)
        hop(long_way(j), 1, j, False)
    for j in (0, 2, 1, 3):
        hop(1 - long_way(j), 2, j, False)
    for step in (1, 2, 3):
        if step > 1:
            for j in (0, 2, 1, 3):
                way = 1 - long_way(j)
                hop_wait(way, step, j)
                hop(way, step + 1, j, True)
        for j in (0, 2, 1, 3):
            way = long_way(j)
            hop_wait(way, step, j)
            hop(way, step + 1, j, True)
    loads[2].wait()
    for j in (0, 2, 1, 3):
        cols = slice(j * WIDE, (j + 1) * WIDE)
        total = part[j, 0]
        for way in (1 - long_way(j), long_way(j)):
            hop_wait(way, 4, j)
            total = total + in_buf[slot(way, 4, j)].astype(F32)
        result[:, cols] = (lat_v[:, cols].astype(F32) + mods[2:3, cols] * total).astype(BF16)
    await_bytes(theirs, pair_send.at[0])
    await_bytes(wo_pair, pair_send.at[1])
    for way in (0, 1):
        for step in (1, 2, 3, 4):
            for j in range(CHUNKS):
                if step > 1 or long_way(j) == way:
                    s = slot(way, step, j)
                    await_bytes(out_buf.at[s], out_send.at[s])


def back_kernel(*refs):
    greet((tp_peer,))
    back(*refs)


def run_back(attended, wo, latent, mods):
    dma = pltpu.SemaphoreType.DMA
    slots = 2 * 4 * CHUNKS
    return pl.pallas_call(
        back_kernel,
        out_shape=jax.ShapeDtypeStruct((ROWS, D), BF16),
        in_specs=[ANY, ANY, ANY, VM],
        out_specs=VM,
        scratch_shapes=[
            pltpu.VMEM((HD, HD), BF16),
            pltpu.VMEM((HD, HD), BF16),
            pltpu.VMEM((HD, D), BF16),
            pltpu.VMEM((HD, D), BF16),
            pltpu.VMEM((ROWS, D), BF16),
            pltpu.VMEM((CHUNKS, NZ, ROWS, WIDE), F32),
            pltpu.VMEM((slots, ROWS, WIDE), BF16),
            pltpu.VMEM((slots, ROWS, WIDE), BF16),
            dma((3,)),
            dma((2,)),
            dma((2,)),
            dma((slots,)),
            dma((slots,)),
        ],
        compiler_params=pltpu.CompilerParams(
            collective_id=2, has_side_effects=True, vmem_limit_bytes=40 * 2**20
        ),
        name="back",
    )(attended, wo, latent, mods)


def shards(
    latent, context, condition, context_condition, modulation,
    query_weight, key_weight, value_weight, lambdas, context_lift, head_gain, output_weight,
):
    q, kv_own, ctx_own, mods = run_front(
        latent, context, condition.reshape(32, 128), context_condition.reshape(32, 128),
        modulation, query_weight, key_weight, value_weight,
    )
    attended = run_middle(q, kv_own, ctx_own, context_lift, lambdas, head_gain.reshape(1, HD))
    return run_back(attended, output_weight, latent, mods)


def solution(mesh):
    split = Mesh(mesh.devices.reshape(4, 4, NZ, 2), ("y", "x", "z", "c"))
    sp, tp = ("y", "x"), ("z", "c")
    return jax.shard_map(
        shards,
        mesh=split,
        in_specs=(
            P(sp + tp, None),
            P(sp, None),
            P(),
            P(),
            P(None, sp, tp),
            P(None, tp),
            P(None, tp),
            P(None, tp),
            P(tp),
            P(tp),
            P(),
            P(tp, None),
        ),
        out_specs=P(sp + tp, None),
        check_vma=False,
    )
```

time: 306 us -> 165 us (0.54)
  waiting for transfers between devices: 157 us -> 0 us
  Pallas kernels: 0 us -> 149 us
  matrix products: 33.8 us -> 0 us
  local copies, waits for them, and re-layouts: 39.2 us -> 13.3 us
  starting transfers between devices: 19.7 us -> 0 us
  other arithmetic: 19.6 us -> 0 us
  blocking collectives: 18.6 us -> 0 us
  between operations: 14.6 us -> 1.37 us
    pallas_call x0 -> x3, Pallas kernels: none -> 149 us  [the longest x1 72.1 us: run_middle(): pl.pallas_call(middle_kernel, out_shape=jax.ShapeDtypeStruct((BLOCK, HD),...]
    all_gather x2 -> x0, waiting for transfers between devices: 75.1 us -> none  [the longest x1 41.4 us: shards(): segment = lax.all_gather(packed, SP, axis=0, tiled=True)]
    reduce_scatter x1 -> x0, waiting for transfers between devices: 60.2 us -> none  [shards(): lax.psum_scatter(jnp.dot(attended, output_weight, preferred_element_type=...]
    dot_general x22 -> x0, matrix products: 33.8 us -> none  [the longest x9 10.9 us: absorb(): jnp.einsum('mqhk,khd->mqhd', weights.astype(jnp.bfloat16), value_part, pr...]
    all_to_all x2 -> x0, waiting for transfers between devices: 21.5 us -> none  [from_everyone(): return lax.all_to_all(copies, axis, split_axis=0, concat_axis=0, tiled=True)]
    dynamic_slice x16 -> x0, local copies, waits for them, and re-layouts: 20.8 us -> none  [shards(): lax.scan(one_block, state_now, stacked)[0]]
    all_to_all x2 -> x0, starting transfers between devices: 19.4 us -> none  [from_everyone(): return lax.all_to_all(copies, axis, split_axis=0, concat_axis=0, tiled=True)]
    psum x2 -> x0, blocking collectives: 18.6 us -> none  [by_axis(): return functools.reduce(lax.psum, axes, shard)]
  transfers between devices with their start and end apart: 5 -> 0, of which waited for: 5 -> 0; matrix products, arithmetic and copies ran while one was open for 5% -> 0% of each run, Pallas kernels for 0% -> 0%
where the time goes in v1:
time: 165 us; the launch traced here: 164 us
  Pallas kernels  149 us (90%)
  local copies, waits for them, and re-layouts  13.3 us (8%)
    pallas_call x1, Pallas kernels, run_middle(): pl.pallas_call(middle_kernel, out_shape=jax.ShapeDtypeStruct((BLOCK, HD),...  72.1 us
    pallas_call x1, Pallas kernels, run_front(): pl.pallas_call(front_kernel, out_shape=(jax.ShapeDtypeStruct((BLOCK, HD),...  41.3 us
    pallas_call x1, Pallas kernels, run_back(): pl.pallas_call(back_kernel, out_shape=jax.ShapeDtypeStruct((ROWS, D), BF1...  36.1 us
    unnamed x31, local copies, waits for them, and re-layouts  13.3 us

profile of v1, /device:TPU:1, one launch (start us, length us, event | category | flops | bytes accessed | tf_op | source)
XLA Modules:
  0.0 164.1 jit_solution(303724515584898392)
XLA Ops:
  1.3 0.0 copy-start.1
  1.3 1.6 copy-done.1
  2.9 0.0 copy-start.2
  2.9 1.6 copy-done.2
  4.5 0.0 copy-start.3
  4.5 1.6 copy-done.3
  6.1 0.0 copy-start.4
  6.1 0.9 copy-done.4
  7.0 0.0 copy-start.6
  7.0 1.0 copy-done.6
  8.0 0.0 copy-start.7
  8.0 0.9 copy-done.7
  9.0 0.0 copy-start.8
  9.0 0.9 copy-done.8
  9.9 0.0 copy-start.9
  9.9 0.9 copy-done.9
  10.8 0.0 copy-start.10
  10.8 0.8 copy-done.10
  11.6 0.0 copy-start.11
  11.6 0.8 copy-done.11
  12.5 0.0 copy-start.12
  12.5 0.7 copy-done.12
  13.2 0.7 copy-done.13
  13.9 0.0 copy-start.14
  13.9 0.0 copy-start.5
  13.9 41.3 %front.1 = (bf16[512,256]{1,0:T(8,128)(2,1)S(1)}, bf16[8,64,512]{2,1,0:T(8,128)(2,1)S(1)}, bf16[32,512]{1,0:T(8,128)(2,1)S(1)}, f32[8,4096]{1,0:T(8,128)S(1)}) custom-call(bf16[32,4096]{1,0:T(8,128)(2,1)S(1)} %copy-done.4, bf16[32,4096]{1,0:T(8,128)(2,1)S(1)} %copy-done.7, f32[32,128]{1,0:T(8,128)S(1)} %bitcast.3, f32[32,128]{1,0:T(8,128)S(1)} %bitcast.4, ...), custom_call_target="tpu_custom_call" | custom-call | tf_op jit(solution)/shard_map/front/pallas_call | solution.py:277
  55.2 0.0 copy-done.14
  55.2 72.1 %middle.1.refs_0_ = bf16[512,256]{1,0:T(8,128)(2,1)S(1)} custom-call(bf16[512,256]{1,0:T(8,128)(2,1)S(1)} %get-tuple-element.9.refs_0_, bf16[8,64,512]{2,1,0:T(8,128)(2,1)S(1)} %get-tuple-element.10.refs_1_, bf16[32,512]{1,0:T(8,128)(2,1)S(1)} %get-tuple-element.11.refs_2_, f32[1]{0:T(128)S(6)} %copy.19.refs_3_, f32[1]{0:T(128)S(6)} %copy.18.refs_4_, ...), custom_call_target="tpu_custom_call" | custom-call | tf_op jit(solution)/shard_map/middle/pallas_call | solution.py:491
  127.3 0.0 copy-done
  127.3 0.0 copy-done.5
  127.3 36.1 %back.1 = bf16[32,4096]{1,0:T(8,128)(2,1)S(1)} custom-call(bf16[512,256]{1,0:T(8,128)(2,1)S(1)} %middle.1.refs_0_, bf16[256,4096]{1,0:T(8,128)(2,1)S(1)} %copy-done, bf16[32,4096]{1,0:T(8,128)(2,1)S(1)} %copy-done.5, f32[8,4096]{1,0:T(8,128)S(1)} %get-tuple-element.12.refs_3_), custom_call_target="tpu_custom_call" | custom-call | tf_op jit(solution)/shard_map/back/pallas_call | solution.py:607
  163.4 0.7 copy.20
  (2 shorter events, 0.0 us)
Async XLA Ops:
  1.3 1.6 copy-start.1
  2.9 1.6 copy-start.2
  4.5 1.6 copy-start.3
  6.1 0.9 copy-start.4
  7.0 1.0 copy-start.6
  8.0 0.9 copy-start.7
  9.0 0.9 copy-start.8
  9.9 0.9 copy-start.9
  10.8 0.8 copy-start.10
  11.6 0.8 copy-start.11
  12.5 0.7 copy-start.12
  13.2 0.7 copy-start.13
  13.9 41.3 %copy-start.14 = (f32[256]{0:T(256)S(1)}, f32[256]{0:T(256)}, u32[]{:S(2)}) copy-start(f32[256]{0:T(256)} %param.26) | copy-start | bytes 3076
  13.9 113.4 %copy-start = (bf16[256,4096]{1,0:T(8,128)(2,1)S(1)}, bf16[256,4096]{1,0:T(8,128)(2,1)}, u32[]{:S(2)}) copy-start(bf16[256,4096]{1,0:T(8,128)(2,1)} %refs_1_.3) | copy-start | bytes 6291460
  13.9 113.4 %copy-start.5 = (bf16[32,4096]{1,0:T(8,128)(2,1)S(1)}, bf16[32,4096]{1,0:T(8,128)(2,1)}, u32[]{:S(2)}) copy-start(bf16[32,4096]{1,0:T(8,128)(2,1)} %refs_2_.1) | copy-start | bytes 786436

commit v2 on v1

--- a/solution.py
+++ b/solution.py
@@ -111,7 +111,7 @@
 
 def front(
     latent, context, cond, ctx_cond, modulation, wq, wk, wv, rcos, rsin, ccos, csin,
-    q_out, kv_out, ctx_out, mods,
+    q_out, kv, ctx, mods, ahead,
     lat, wq_v, wk_v, wv_v, mod_v, ctx_v, parts, normed,
     load, mod_send, mod_recv, ring_send, ring_recv, pair_send, pair_recv,
 ):
@@ -230,11 +230,15 @@
             q = turned(q_raw[part].astype(F32), cos, sin)
             for core in (0, 1):
                 q_out[core * HD + o * ROWS : core * HD + (o + 1) * ROWS, :] = q[core * ROWS : (core + 1) * ROWS]
-            kv_out[o, :, 0:HD] = turned(k_raw[part].astype(F32), cos, sin)
-            kv_out[o, :, HD : 2 * HD] = v_raw[part]
+            here = pl.ds(pl.multiple_of(sp * UNIT, UNIT), UNIT)
+            kv[o, here, 0:HD] = turned(k_raw[part].astype(F32), cos, sin)
+            kv[o, here, HD : 2 * HD] = v_raw[part]
         if with_context:
-            ctx_out[:, 0:HD] = k_raw[count * UNIT : end]
-            ctx_out[:, HD : 2 * HD] = v_raw[count * UNIT : end]
+            for o in range(2):
+                here = pl.ds(pl.multiple_of(sp * 16, 16), 16)
+                part = slice(count * UNIT + o * 16, count * UNIT + o * 16 + 16)
+                ctx[o, here, 0:HD] = k_raw[part]
+                ctx[o, here, HD : 2 * HD] = v_raw[part]
 
     forward(1)
     await_bytes(mods.at[:, pl.ds(0, (NS - 1) * HD)], mod_recv.at[1])
@@ -242,22 +246,27 @@
         copy.wait()
     pair_wait(0)
     project([0], True)
+    ahead(0)
     forward(2)
     for rel in (7, 1):
         pair_wait(rel)
     project([7, 1], False)
+    ahead(1)
     forward(3)
     for rel in (6, 2):
         pair_wait(rel)
     project([6, 2], False)
+    ahead(2)
     ring_wait(4, 0)
     ring_wait(4, 1)
     pair_step(4)
     for rel in (5, 3):
         pair_wait(rel)
     project([5, 3], False)
+    ahead(3)
     pair_wait(4)
     project([4], False)
+    ahead(4)
 
     await_bytes(parts.at[pl.ds(0, NS - 1)], mod_send.at[0])
     await_bytes(mods.at[:, pl.ds(0, (NS - 1) * HD)], mod_send.at[1])
@@ -267,48 +276,7 @@
         await_bytes(lat.at[0, 0], pair_send.at[rel])
 
 
-def front_kernel(*refs):
-    greet((sp_peer, tp_peer))
-    front(*refs)
-
-
-def run_front(latent, context, cond, ctx_cond, modulation, wq, wk, wv):
-    dma = pltpu.SemaphoreType.DMA
-    return pl.pallas_call(
-        front_kernel,
-        out_shape=(
-            jax.ShapeDtypeStruct((BLOCK, HD), BF16),
-            jax.ShapeDtypeStruct((NZ, UNIT, 2 * HD), BF16),
-            jax.ShapeDtypeStruct((ROWS, 2 * HD), BF16),
-            jax.ShapeDtypeStruct((8, D), F32),
-        ),
-        in_specs=[ANY, ANY, VM, VM, ANY, ANY, ANY, ANY, VM, VM, VM, VM],
-        out_specs=(VM, VM, VM, VM),
-        scratch_shapes=[
-            pltpu.VMEM((NZ, 2, ROWS, D), BF16),
-            pltpu.VMEM((D, HD), BF16),
-            pltpu.VMEM((D, HD), BF16),
-            pltpu.VMEM((D, HD), BF16),
-            pltpu.VMEM((3, HD, HD), BF16),
-            pltpu.VMEM((ROWS, D), BF16),
-            pltpu.VMEM((NS, 8, HD), F32),
-            pltpu.VMEM((2 * UNIT, D), BF16),
-            dma((6,)),
-            dma((2,)),
-            dma((2,)),
-            dma((2 * NZ,)),
-            dma((2 * NZ,)),
-            dma((NZ,)),
-            dma((NZ,)),
-        ],
-        compiler_params=pltpu.CompilerParams(
-            collective_id=0, has_side_effects=True, vmem_limit_bytes=40 * 2**20
-        ),
-        name="front",
-    )(latent, context, cond, ctx_cond, modulation, wq, wk, wv, *[jnp.asarray(t) for t in tables()])
-
-
-def gather_unit(kv, kv_send, kv_recv):
+def gather_unit(kv, tall, kv_send, kv_recv):
     y, x, z, c = position()
 
     def geometry(o):
@@ -327,11 +295,11 @@
 
         oy, ox = pair(first + df, second + dg)
         ty, tx = pair(first + tf, second + tg)
-        rows = pl.ds(pl.multiple_of((oy * 4 + ox) * UNIT, UNIT), UNIT)
+        rows = pl.ds(pl.multiple_of((oy * 4 + ox) * tall, tall), tall)
         send(kv.at[o, rows], kv.at[o, rows], kv_send.at[0], kv_recv.at[o * 5 + kind], (ty, tx, z, c))
 
     def wait(o, kind, count):
-        await_bytes(kv.at[o, pl.ds(0, count * UNIT)], kv_recv.at[o * 5 + kind])
+        await_bytes(kv.at[o, pl.ds(0, count * tall)], kv_recv.at[o * 5 + kind])
 
     def own(o):
         geo = geometry(o)
@@ -375,141 +343,25 @@
         wait(o, 4, 8)
 
     def all_sent():
-        for _ in range(NS - 1):
-            await_bytes(kv.at[0, pl.ds(0, NZ * UNIT)], kv_send.at[0])
+        await_bytes(kv.at[:, pl.ds(0, (NS - 1) * tall)], kv_send.at[0])
 
     return own, (stage1, stage2, stage3, stage4), done, all_sent
 
 
-def absorb(q, key_part, value_part, lift, peak, sums, acc):
-    factor = PART**-0.5 * LOG2E
-    values = value_part()
-    for m in range(2):
-        scores = lax.dot_general(
-            q[:, m * PART : (m + 1) * PART], key_part(m), (((1,), (1,)), ((), ())), preferred_element_type=F32
-        )
-        scores = scores * factor
-        if lift is not None:
-            scores = scores + lift
-        before = peak[m]
-        now = jnp.maximum(before, jnp.max(scores, axis=1, keepdims=True))
-        fading = jnp.exp2(before - now)
-        weights = jnp.exp2(scores - now[:, 0:1])
-        sums[m] = sums[m] * fading + jnp.sum(weights, axis=1, keepdims=True)
-        acc[m] = acc[m] * fading[:, 0:1] + jnp.dot(
-            weights.astype(BF16), values, preferred_element_type=F32
-        )
-        peak[m] = now
-
-
-def middle(
-    q, kv_own, ctx_own, lift, lam, gain,
-    attended,
-    kv, ctx, peak, sums, acc,
-    load, ctx_send, ctx_recv, kv_send, kv_recv,
-):
-    y, x, z, c = position()
-    sp = y * 4 + x
-    loads = [
-        pltpu.make_async_copy(kv_own, kv.at[:, pl.ds(pl.multiple_of(sp * UNIT, UNIT), UNIT)], load.at[0]),
-        pltpu.make_async_copy(ctx_own, ctx.at[pl.ds(pl.multiple_of(sp * ROWS, ROWS), ROWS)], load.at[1]),
-    ]
-    for copy in loads:
-        copy.start()
-    peak[...] = jnp.full(peak.shape, -jnp.inf, F32)
-    sums[...] = jnp.zeros(sums.shape, F32)
-    acc[...] = jnp.zeros(acc.shape, F32)
-    own, stages, done, all_sent = gather_unit(kv, kv_send, kv_recv)
-    for copy in loads:
-        copy.wait()
-    greeted((sp_peer,))
-
-    def show_context(i, carry):
-        mine = ctx.at[pl.ds(pl.multiple_of(sp * ROWS, ROWS), ROWS)]
-        send(mine, mine, ctx_send.at[0], ctx_recv.at[0], sp_peer(i))
-        return carry
-
-    lax.fori_loop(1, NS, show_context, 0)
-
-    def start_own(o, carry):
-        own(o)
-        return carry
-
-    lax.fori_loop(0, NZ, start_own, 0)
-    lift_term = lift[0] * LOG2E
-
-    def tick(t, carry):
-        for back, stage in enumerate(stages):
-            o = t - back
-
-            @pl.when((o >= 0) & (o < NZ))
-            def _():
-                stage(o)
-
-        @pl.when(t == 1)
-        def _():
-            await_bytes(ctx.at[pl.ds(0, (NS - 1) * ROWS)], ctx_recv.at[0])
-            absorb(
-                q, lambda m: ctx[:, m * PART : (m + 1) * PART], lambda: ctx[:, HD : 2 * HD],
-                lift_term, peak, sums, acc,
-            )
-
-        o = t - len(stages)
-
-        @pl.when(o >= 0)
-        def _():
-            done(o)
-
-            def part(i, inner):
-                rows = pl.ds(pl.multiple_of(i * 512, 512), 512)
-                absorb(
-                    q, lambda m: kv[o, rows, m * PART : (m + 1) * PART], lambda: kv[o, rows, HD : 2 * HD],
-                    None, peak, sums, acc,
-                )
-                return inner
-
-            lax.fori_loop(0, 2, part, 0)
-
-        return carry
-
-    lax.fori_loop(0, NZ + len(stages), tick, 0)
-    means = [acc[m] / sums[m][:, 0:1] for m in range(2)]
-    difference = means[0] - lam[0] * means[1]
-    spread = jnp.mean(difference * difference, axis=1, keepdims=True)
-    attended[...] = (difference * lax.rsqrt(spread + EPS) * gain[...]).astype(BF16)
-    all_sent()
-    await_bytes(ctx.at[pl.ds(0, (NS - 1) * ROWS)], ctx_send.at[0])
-
-
-def middle_kernel(*refs):
-    greet((sp_peer,))
-    middle(*refs)
-
-
-def run_middle(q, kv_own, ctx_own, lift, lam, gain):
-    dma = pltpu.SemaphoreType.DMA
-    return pl.pallas_call(
-        middle_kernel,
-        out_shape=jax.ShapeDtypeStruct((BLOCK, HD), BF16),
-        in_specs=[VM, ANY, ANY, SM, SM, VM],
-        out_specs=VM,
-        scratch_shapes=[
-            pltpu.VMEM((NZ, NS * UNIT, 2 * HD), BF16),
-            pltpu.VMEM((NS * ROWS, 2 * HD), BF16),
-            pltpu.VMEM((2, BLOCK, 128), F32),
-            pltpu.VMEM((2, BLOCK, 128), F32),
-            pltpu.VMEM((2, BLOCK, HD), F32),
-            dma((2,)),
-            dma((1,)),
-            dma((1,)),
-            dma((1,)),
-            dma((5 * NZ,)),
-        ],
-        compiler_params=pltpu.CompilerParams(
-            collective_id=1, has_side_effects=True, vmem_limit_bytes=40 * 2**20
-        ),
-        name="middle",
-    )(q, kv_own, ctx_own, lift, lam, gain)
+def absorb(q, m, keys, values, lift, peak, sums, acc):
+    scores = lax.dot_general(
+        q[:, m * PART : (m + 1) * PART], keys, (((1,), (1,)), ((), ())), preferred_element_type=F32
+    )
+    scores = scores * (PART**-0.5 * LOG2E)
+    if lift is not None:
+        scores = scores + lift
+    before = peak[m]
+    now = jnp.maximum(before, jnp.max(scores, axis=1, keepdims=True))
+    fading = jnp.exp2(before - now)
+    weights = jnp.exp2(scores - now[:, 0:1])
+    sums[m] = sums[m] * fading + jnp.sum(weights, axis=1, keepdims=True)
+    acc[m] = acc[m] * fading[:, 0:1] + jnp.dot(weights.astype(BF16), values, preferred_element_type=F32)
+    peak[m] = now
 
 
 CHUNKS = 4
@@ -517,25 +369,15 @@
 
 
 def back(
-    attended, wo, latent, mods,
+    attended, lat, mods,
     result,
-    mine, theirs, wo_v, wo_pair, lat_v, part, out_buf, in_buf,
-    load, pair_send, pair_recv, out_send, out_recv,
+    theirs, wo_v, wo_pair, part, out_buf, in_buf,
+    pair_send, pair_recv, out_send, out_recv,
 ):
     y, x, z, c = position()
     pair = (y, x, z, 1 - c)
-    loads = [
-        pltpu.make_async_copy(wo, wo_v, load.at[0]),
-        pltpu.make_async_copy(attended.at[pl.ds(pl.multiple_of(c * HD, HD), HD)], mine, load.at[1]),
-        pltpu.make_async_copy(latent, lat_v, load.at[2]),
-    ]
-    for copy in loads:
-        copy.start()
-    greeted((tp_peer,))
-    send(attended.at[pl.ds(pl.multiple_of((1 - c) * HD, HD), HD)], theirs, pair_send.at[0], pair_recv.at[0], pair)
-    loads[0].wait()
-    send(wo_v, wo_pair, pair_send.at[1], pair_recv.at[1], pair)
-    loads[1].wait()
+    send(attended.at[1 - c], theirs, pair_send.at[0], pair_recv.at[0], pair)
+    mine = attended[c]
     await_bytes(theirs, pair_recv.at[0])
     await_bytes(wo_pair, pair_recv.at[1])
 
@@ -561,7 +403,7 @@
 
     for j in (0, 2, 1, 3):
         cols = slice(j * WIDE, (j + 1) * WIDE)
-        product = jnp.dot(mine[...], wo_v[:, cols], preferred_element_type=F32) + jnp.dot(
+        product = jnp.dot(mine, wo_v[:, cols], preferred_element_type=F32) + jnp.dot(
             theirs[...], wo_pair[:, cols], preferred_element_type=F32
         )
         part[j] = product.reshape(NZ, ROWS, WIDE)
@@ -578,14 +420,13 @@
             way = long_way(j)
             hop_wait(way, step, j)
             hop(way, step + 1, j, True)
-    loads[2].wait()
     for j in (0, 2, 1, 3):
         cols = slice(j * WIDE, (j + 1) * WIDE)
         total = part[j, 0]
         for way in (1 - long_way(j), long_way(j)):
             hop_wait(way, 4, j)
             total = total + in_buf[slot(way, 4, j)].astype(F32)
-        result[:, cols] = (lat_v[:, cols].astype(F32) + mods[2:3, cols] * total).astype(BF16)
+        result[:, cols] = (lat[z, c, :, cols].astype(F32) + mods[2:3, cols] * total).astype(BF16)
     await_bytes(theirs, pair_send.at[0])
     await_bytes(wo_pair, pair_send.at[1])
     for way in (0, 1):
@@ -596,51 +437,177 @@
                     await_bytes(out_buf.at[s], out_send.at[s])
 
 
-def back_kernel(*refs):
-    greet((tp_peer,))
-    back(*refs)
-
-
-def run_back(attended, wo, latent, mods):
+def kernel(
+    latent, context, cond, ctx_cond, modulation, wq, wk, wv, rcos, rsin, ccos, csin, lift, lam, gain, wo,
+    result,
+    lat, wq_v, wk_v, wv_v, mod_v, ctx_v, parts, normed, mods,
+    q, kv, ctx, peak, sums, acc, attended,
+    theirs, wo_v, wo_pair, part, out_buf, in_buf,
+    load, mod_send, mod_recv, ring_send, ring_recv, pair_send, pair_recv,
+    kv_send, kv_recv, ctx_send, ctx_recv,
+    back_load, back_send, back_recv, out_send, out_recv,
+):
+    y, x, z, c = position()
+    greet((sp_peer, tp_peer))
+    wo_copy = pltpu.make_async_copy(wo, wo_v, back_load.at[0])
+    own, stages, done, all_sent = gather_unit(kv, UNIT, kv_send, kv_recv)
+    ctx_own, ctx_stages, ctx_done, ctx_all_sent = gather_unit(ctx, 16, ctx_send, ctx_recv)
+    peak[...] = jnp.full(peak.shape, -jnp.inf, F32)
+    sums[...] = jnp.zeros(sums.shape, F32)
+    acc[...] = jnp.zeros(acc.shape, F32)
+
+    def over(count, one, first=0):
+        lax.fori_loop(first, first + count, lambda o, carry: (one(o), carry)[1], 0)
+
+    def ahead(step):
+        if step == 0:
+            own(0)
+            over(2, ctx_own)
+            wo_copy.start()
+        if step == 1:
+            over(2, own, 1)
+            over(2, ctx_stages[0])
+            stages[0](0)
+            wo_copy.wait()
+            send(wo_v, wo_pair, back_send.at[1], back_recv.at[1], (y, x, z, 1 - c))
+        if step == 2:
+            over(2, own, 3)
+            over(2, ctx_stages[1])
+            stages[0](1)
+            stages[1](0)
+        if step == 3:
+            over(2, own, 5)
+            over(2, ctx_stages[2])
+            over(2, ctx_stages[3])
+            stages[0](2)
+            stages[1](1)
+            stages[2](0)
+        if step == 4:
+            own(7)
+
+    front(
+        latent, context, cond, ctx_cond, modulation, wq, wk, wv, rcos, rsin, ccos, csin,
+        q, kv, ctx, mods, ahead,
+        lat, wq_v, wk_v, wv_v, mod_v, ctx_v, parts, normed,
+        load, mod_send, mod_recv, ring_send, ring_recv, pair_send, pair_recv,
+    )
+    lift_term = lift[0] * LOG2E
+    lag = 5
+
+    def tick(t, carry):
+        def stage(k):
+            o = t - k
+
+            @pl.when((o >= 0) & (o < NZ))
+            def _():
+                stages[k](o)
+
+        def attend(m):
+            o = t - lag
+
+            @pl.when(o >= 0)
+            def _():
+                if m == 0:
+                    done(o)
+                absorb(q, m, kv[o, :, m * PART : (m + 1) * PART], kv[o, :, HD : 2 * HD], None, peak, sums, acc)
+
+        stage(0)
+        attend(0)
+        stage(1)
+        stage(2)
+        attend(1)
+        stage(3)
+
+        @pl.when(t == 3)
+        def _():
+            over(2, ctx_done)
+            for m in range(2):
+                absorb(
+                    q, m, ctx[:, :, m * PART : (m + 1) * PART].reshape(NS * ROWS, PART),
+                    ctx[:, :, HD : 2 * HD].reshape(NS * ROWS, HD), lift_term, peak, sums, acc,
+                )
+
+        return carry
+
+    lax.fori_loop(3, NZ + lag, tick, 0)
+    means = [acc[m] / sums[m][:, 0:1] for m in range(2)]
+    difference = means[0] - lam[0] * means[1]
+    spread = jnp.mean(difference * difference, axis=1, keepdims=True)
+    final = (difference * lax.rsqrt(spread + EPS) * gain[...]).astype(BF16)
+    attended[0] = final[0:HD]
+    attended[1] = final[HD : 2 * HD]
+    back(
+        attended, lat, mods, result, theirs, wo_v, wo_pair, part, out_buf, in_buf,
+        back_send, back_recv, out_send, out_recv,
+    )
+    all_sent()
+    ctx_all_sent()
+
+
+def run(*arrays):
     dma = pltpu.SemaphoreType.DMA
     slots = 2 * 4 * CHUNKS
     return pl.pallas_call(
-        back_kernel,
+        kernel,
         out_shape=jax.ShapeDtypeStruct((ROWS, D), BF16),
-        in_specs=[ANY, ANY, ANY, VM],
+        in_specs=[ANY, ANY, VM, VM, ANY, ANY, ANY, ANY, VM, VM, VM, VM, SM, SM, VM, ANY],
         out_specs=VM,
         scratch_shapes=[
-            pltpu.VMEM((HD, HD), BF16),
+            pltpu.VMEM((NZ, 2, ROWS, D), BF16),
+            pltpu.VMEM((D, HD), BF16),
+            pltpu.VMEM((D, HD), BF16),
+            pltpu.VMEM((D, HD), BF16),
+            pltpu.VMEM((3, HD, HD), BF16),
+            pltpu.VMEM((ROWS, D), BF16),
+            pltpu.VMEM((NS, 8, HD), F32),
+            pltpu.VMEM((2 * UNIT, D), BF16),
+            pltpu.VMEM((8, D), F32),
+            pltpu.VMEM((BLOCK, HD), BF16),
+            pltpu.VMEM((NZ, NS * UNIT, 2 * HD), BF16),
+            pltpu.VMEM((2, NS * 16, 2 * HD), BF16),
+            pltpu.VMEM((2, BLOCK, 128), F32),
+            pltpu.VMEM((2, BLOCK, 128), F32),
+            pltpu.VMEM((2, BLOCK, HD), F32),
+            pltpu.VMEM((2, HD, HD), BF16),
             pltpu.VMEM((HD, HD), BF16),
             pltpu.VMEM((HD, D), BF16),
             pltpu.VMEM((HD, D), BF16),
-            pltpu.VMEM((ROWS, D), BF16),
             pltpu.VMEM((CHUNKS, NZ, ROWS, WIDE), F32),
             pltpu.VMEM((slots, ROWS, WIDE), BF16),
             pltpu.VMEM((slots, ROWS, WIDE), BF16),
-            dma((3,)),
+            dma((6,)),
+            dma((2,)),
+            dma((2,)),
+            dma((2 * NZ,)),
+            dma((2 * NZ,)),
+            dma((NZ,)),
+            dma((NZ,)),
+            dma((1,)),
+            dma((5 * NZ,)),
+            dma((1,)),
+            dma((10,)),
+            dma((1,)),
             dma((2,)),
             dma((2,)),
             dma((slots,)),
             dma((slots,)),
         ],
         compiler_params=pltpu.CompilerParams(
-            collective_id=2, has_side_effects=True, vmem_limit_bytes=40 * 2**20
+            collective_id=0, has_side_effects=True, vmem_limit_bytes=60 * 2**20
         ),
-        name="back",
-    )(attended, wo, latent, mods)
+        name="whole",
+    )(*arrays)
 
 
 def shards(
     latent, context, condition, context_condition, modulation,
     query_weight, key_weight, value_weight, lambdas, context_lift, head_gain, output_weight,
 ):
-    q, kv_own, ctx_own, mods = run_front(
+    return run(
         latent, context, condition.reshape(32, 128), context_condition.reshape(32, 128),
-        modulation, query_weight, key_weight, value_weight,
+        modulation, query_weight, key_weight, value_weight, *[jnp.asarray(t) for t in tables()],
+        context_lift, lambdas, head_gain.reshape(1, HD), output_weight,
     )
-    attended = run_middle(q, kv_own, ctx_own, context_lift, lambdas, head_gain.reshape(1, HD))
-    return run_back(attended, output_weight, latent, mods)
 
 
 def solution(mesh):

time: 165 us -> 121 us (0.73)
  Pallas kernels: 149 us -> 118 us
  local copies, waits for them, and re-layouts: 13.3 us -> 1.67 us
    pallas_call x3 -> x1, Pallas kernels: 149 us -> 118 us  [run(): pl.pallas_call(kernel, out_shape=jax.ShapeDtypeStruct((ROWS, D), BF16), i...]
    unnamed x31 -> x1, local copies, waits for them, and re-layouts: 13.3 us -> 1.67 us
where the time goes in v2:
time: 121 us
  Pallas kernels  118 us (98%)
  local copies, waits for them, and re-layouts  1.67 us (1%)
  between operations  1.31 us (1%)
    pallas_call x1, Pallas kernels, run(): pl.pallas_call(kernel, out_shape=jax.ShapeDtypeStruct((ROWS, D), BF16), i...  118 us

profile of v2, /device:TPU:1, one launch (start us, length us, event | category | flops | bytes accessed | tf_op | source)
XLA Modules:
  0.0 120.6 jit_solution(17598520021967776229)
XLA Ops:
  1.3 117.6 %whole.1 = bf16[32,4096]{1,0:T(8,128)(2,1)} custom-call(bf16[32,4096]{1,0:T(8,128)(2,1)} %latent.1, bf16[32,4096]{1,0:T(8,128)(2,1)} %context.1, f32[32,128]{1,0:T(8,128)} %bitcast.3, f32[32,128]{1,0:T(8,128)} %bitcast.4, bf16[3,256,256]{2,1,0:T(8,128)(2,1)} %modulation.1, bf16[4096,256]{1,0:T(8,128)(2,1)} %wq.1, bf16[4096,256]{1,0:T(8,128)(2,1)} %wk.1, ...), custom_call_target="tpu_custom_call" | custom-call | tf_op jit(solution)/shard_map/whole/pallas_call | solution.py:550
  118.9 1.7 %copy.20 = bf16[32,4096]{1,0:T(8,128)(2,1)} copy(bf16[32,4096]{1,0:T(8,128)(2,1)} %whole.1) | data formatting | bytes 524288

commit v3 on v2

--- a/solution.py
+++ b/solution.py
@@ -25,6 +25,7 @@
 ORDER = (0, 7, 1, 6, 2, 5, 3, 4)
 PLACE = {rel: i for i, rel in enumerate(ORDER)}
 UNIT = 2 * ROWS
+SLOTS_AHEAD = (0, 0, 2, 3, 4, 5)
 BLOCK = NZ * UNIT
 ANY = pl.BlockSpec(memory_space=pl.ANY)
 VM = pl.BlockSpec(memory_space=pltpu.VMEM)
@@ -58,8 +59,12 @@
         lax.fori_loop(1, NS, one, 0)
 
 
+    y, x, z, c = position()
+    pl.semaphore_signal(barrier, inc=1, device_id=(y, 3 - x, z, 1 - c), device_id_type=MESH)
+
+
 def greeted(peers):
-    pl.semaphore_wait(pltpu.get_barrier_semaphore(), (NS - 1) * len(peers))
+    pl.semaphore_wait(pltpu.get_barrier_semaphore(), (NS - 1) * len(peers) + 1)
 
 
 def send(src, dst, send_sem, recv_sem, to):
@@ -111,12 +116,14 @@
 
 def front(
     latent, context, cond, ctx_cond, modulation, wq, wk, wv, rcos, rsin, ccos, csin,
-    q_out, kv, ctx, mods, ahead,
+    q, kv, ctx, kv_away, ctx_away, mods, ahead, early,
     lat, wq_v, wk_v, wv_v, mod_v, ctx_v, parts, normed,
     load, mod_send, mod_recv, ring_send, ring_recv, pair_send, pair_recv,
 ):
     y, x, z, c = position()
     sp, tp = y * 4 + x, z * 2 + c
+    right = c == x // 2
+    seat = lax.rem(x, 2) * 4 + y
     loads = [
         pltpu.make_async_copy(latent, lat.at[z, c], load.at[0]),
         pltpu.make_async_copy(modulation, mod_v, load.at[1]),
@@ -155,6 +162,7 @@
 
     loads[0].wait()
     greeted((sp_peer, tp_peer))
+    early()
     for half in (0, 1):
         for way in (1, -1):
             ring_step(1, way, half)
@@ -227,27 +235,41 @@
             cos = rcos[line, :] + ccos[...]
             sin = rsin[line, :] + csin[...]
             part = slice(i * UNIT, (i + 1) * UNIT)
-            q = turned(q_raw[part].astype(F32), cos, sin)
-            for core in (0, 1):
-                q_out[core * HD + o * ROWS : core * HD + (o + 1) * ROWS, :] = q[core * ROWS : (core + 1) * ROWS]
-            here = pl.ds(pl.multiple_of(sp * UNIT, UNIT), UNIT)
-            kv[o, here, 0:HD] = turned(k_raw[part].astype(F32), cos, sin)
-            kv[o, here, HD : 2 * HD] = v_raw[part]
+            q[0, o * UNIT : (o + 1) * UNIT, :] = turned(q_raw[part].astype(F32), cos, sin)
+            keys = turned(k_raw[part].astype(F32), cos, sin)
+
+            @pl.when(right)
+            def _():
+                here = pl.ds(pl.multiple_of(seat * UNIT, UNIT), UNIT)
+                kv[c, o, here, 0:HD] = keys
+                kv[c, o, here, HD : 2 * HD] = v_raw[part]
+
+            @pl.when(jnp.logical_not(right))
+            def _():
+                kv_away[o, :, 0:HD] = keys
+                kv_away[o, :, HD : 2 * HD] = v_raw[part]
+
         if with_context:
-            for o in range(2):
-                here = pl.ds(pl.multiple_of(sp * 16, 16), 16)
-                part = slice(count * UNIT + o * 16, count * UNIT + o * 16 + 16)
-                ctx[o, here, 0:HD] = k_raw[part]
-                ctx[o, here, HD : 2 * HD] = v_raw[part]
+
+            @pl.when(right)
+            def _():
+                here = pl.ds(pl.multiple_of(seat * ROWS, ROWS), ROWS)
+                ctx[c, 0, here, 0:HD] = k_raw[count * UNIT : end]
+                ctx[c, 0, here, HD : 2 * HD] = v_raw[count * UNIT : end]
+
+            @pl.when(jnp.logical_not(right))
+            def _():
+                ctx_away[:, 0:HD] = k_raw[count * UNIT : end]
+                ctx_away[:, HD : 2 * HD] = v_raw[count * UNIT : end]
 
     forward(1)
+    forward(2)
     await_bytes(mods.at[:, pl.ds(0, (NS - 1) * HD)], mod_recv.at[1])
     for copy in loads[2:]:
         copy.wait()
     pair_wait(0)
     project([0], True)
     ahead(0)
-    forward(2)
     for rel in (7, 1):
         pair_wait(rel)
     project([7, 1], False)
@@ -278,79 +300,100 @@
 
 def gather_unit(kv, tall, kv_send, kv_recv):
     y, x, z, c = position()
-
-    def geometry(o):
-        swap = lax.rem(o, 2)
-        way = 1 - 2 * lax.rem(o // 2, 2)
-        first = swap * y + (1 - swap) * x
-        second = swap * x + (1 - swap) * y
-        return swap, way, first, second
-
-    def step(o, geo, df, dg, tf, tg, kind):
-        swap, way, first, second = geo
-
-        def pair(f, g):
-            f, g = lax.rem(f + 8, 4), lax.rem(g + 8, 4)
-            return swap * f + (1 - swap) * g, swap * g + (1 - swap) * f
-
-        oy, ox = pair(first + df, second + dg)
-        ty, tx = pair(first + tf, second + tg)
-        rows = pl.ds(pl.multiple_of((oy * 4 + ox) * tall, tall), tall)
-        send(kv.at[o, rows], kv.at[o, rows], kv_send.at[0], kv_recv.at[o * 5 + kind], (ty, tx, z, c))
-
-    def wait(o, kind, count):
-        await_bytes(kv.at[o, pl.ds(0, count * tall)], kv_recv.at[o * 5 + kind])
+    mate = x + 1 - 2 * lax.rem(x, 2)
+
+    def wrap(v):
+        return lax.rem(v + 8, 4)
+
+    def way_of(o):
+        return 1 - 2 * lax.rem(o // 2, 2)
+
+    def step(o, crossed, dy, over, ty, kind):
+        ox = mate if crossed else x
+        seat = lax.rem(ox, 2) * 4 + wrap(y + dy)
+        rows = pl.ds(pl.multiple_of(seat * tall, tall), tall)
+        send(
+            kv.at[c, o, rows], kv.at[c, o, rows], kv_send.at[0], kv_recv.at[o * 4 + kind],
+            (wrap(y + ty), mate if over else x, z, c),
+        )
+
+    def wait(o, kind, count=1):
+        await_bytes(kv.at[c, o, pl.ds(0, count * tall)], kv_recv.at[o * 4 + kind])
+
+    def typed(o, even, odd):
+        if isinstance(o, int):
+            (odd if o % 2 else even)()
+        else:
+            pl.when(lax.rem(o, 2) == 0)(even)
+            pl.when(lax.rem(o, 2) == 1)(odd)
 
     def own(o):
-        geo = geometry(o)
-        way = geo[1]
-        step(o, geo, 0, 0, 1, 0, 0)
-        step(o, geo, 0, 0, -1, 0, 0)
-        step(o, geo, 0, 0, 0, way, 1)
-        step(o, geo, 0, 0, 0, -way, 4)
+        way = way_of(o)
+
+        def even():
+            step(o, False, 0, True, 0, 0)
+            step(o, False, 0, False, way, 1)
+            step(o, False, 0, False, -way, 3)
+
+        def odd():
+            step(o, False, 0, False, way, 1)
+            step(o, False, 0, False, -way, 0)
+            step(o, False, 0, True, 0, 3)
+
+        typed(o, even, odd)
 
     def stage1(o):
-        geo = geometry(o)
-        way = geo[1]
-        wait(o, 0, 2)
-        step(o, geo, -way, 0, way, 0, 1)
-        for d in (1, -1):
-            step(o, geo, d, 0, 0, way, 2)
-            step(o, geo, d, 0, 0, -way, 4)
+        way = way_of(o)
+
+        def even():
+            wait(o, 0)
+            step(o, True, 0, False, way, 2)
+            step(o, True, 0, False, -way, 3)
+
+        def odd():
+            wait(o, 1)
+            step(o, False, -way, False, way, 2)
+            step(o, False, -way, True, 0, 3)
+            wait(o, 0)
+            step(o, False, way, True, 0, 3)
+
+        typed(o, even, odd)
 
     def stage2(o):
-        geo = geometry(o)
-        way = geo[1]
-        wait(o, 1, 2)
-        step(o, geo, 2, 0, 0, way, 3)
-        step(o, geo, 2, 0, 0, -way, 4)
-        step(o, geo, 0, -way, 0, way, 4)
+        way = way_of(o)
+
+        def even():
+            wait(o, 1)
+            step(o, False, -way, False, way, 3)
+
+        def odd():
+            wait(o, 2)
+            step(o, False, 2, True, 0, 3)
+
+        typed(o, even, odd)
 
     def stage3(o):
-        geo = geometry(o)
-        way = geo[1]
-        wait(o, 2, 2)
-        for d in (1, -1):
-            step(o, geo, d, -way, 0, way, 4)
-
-    def stage4(o):
-        geo = geometry(o)
-        way = geo[1]
-        wait(o, 3, 1)
-        step(o, geo, 2, -way, 0, way, 4)
+        way = way_of(o)
+
+        def even():
+            wait(o, 2)
+            step(o, True, -way, False, way, 3)
+
+        typed(o, even, lambda: None)
 
     def done(o):
-        wait(o, 4, 8)
-
-    def all_sent():
-        await_bytes(kv.at[:, pl.ds(0, (NS - 1) * tall)], kv_send.at[0])
-
-    return own, (stage1, stage2, stage3, stage4), done, all_sent
+        wait(o, 3, 4)
+
+    def all_sent(units):
+        for o in range(units):
+            await_bytes(kv.at[0, 0, pl.ds(0, 7 * tall)], kv_send.at[0])
+
+    return own, (stage1, stage2, stage3), done, all_sent
 
 
 def absorb(q, m, keys, values, lift, peak, sums, acc):
     scores = lax.dot_general(
-        q[:, m * PART : (m + 1) * PART], keys, (((1,), (1,)), ((), ())), preferred_element_type=F32
+        q, keys, (((1,), (1,)), ((), ())), preferred_element_type=F32
     )
     scores = scores * (PART**-0.5 * LOG2E)
     if lift is not None:
@@ -369,16 +412,13 @@
 
 
 def back(
-    attended, lat, mods,
+    heads, lat, mods,
     result,
-    theirs, wo_v, wo_pair, part, out_buf, in_buf,
+    wo_v, wo_pair, part, out_buf, in_buf,
     pair_send, pair_recv, out_send, out_recv,
 ):
     y, x, z, c = position()
-    pair = (y, x, z, 1 - c)
-    send(attended.at[1 - c], theirs, pair_send.at[0], pair_recv.at[0], pair)
-    mine = attended[c]
-    await_bytes(theirs, pair_recv.at[0])
+    mine, theirs = heads[0], heads[1]
     await_bytes(wo_pair, pair_recv.at[1])
 
     def long_way(j):
@@ -404,7 +444,7 @@
     for j in (0, 2, 1, 3):
         cols = slice(j * WIDE, (j + 1) * WIDE)
         product = jnp.dot(mine, wo_v[:, cols], preferred_element_type=F32) + jnp.dot(
-            theirs[...], wo_pair[:, cols], preferred_element_type=F32
+            theirs, wo_pair[:, cols], preferred_element_type=F32
         )
         part[j] = product.reshape(NZ, ROWS, WIDE)
         hop(long_way(j), 1, j, False)
@@ -427,7 +467,6 @@
             hop_wait(way, 4, j)
             total = total + in_buf[slot(way, 4, j)].astype(F32)
         result[:, cols] = (lat[z, c, :, cols].astype(F32) + mods[2:3, cols] * total).astype(BF16)
-    await_bytes(theirs, pair_send.at[0])
     await_bytes(wo_pair, pair_send.at[1])
     for way in (0, 1):
         for step in (1, 2, 3, 4):
@@ -441,107 +480,199 @@
     latent, context, cond, ctx_cond, modulation, wq, wk, wv, rcos, rsin, ccos, csin, lift, lam, gain, wo,
     result,
     lat, wq_v, wk_v, wv_v, mod_v, ctx_v, parts, normed, mods,
-    q, kv, ctx, peak, sums, acc, attended,
-    theirs, wo_v, wo_pair, part, out_buf, in_buf,
+    q, kv, ctx, kv_away, ctx_away, settings, peak, sums, acc, attended, heads,
+    wo_v, wo_pair, part, out_buf, in_buf,
     load, mod_send, mod_recv, ring_send, ring_recv, pair_send, pair_recv,
-    kv_send, kv_recv, ctx_send, ctx_recv,
-    back_load, back_send, back_recv, out_send, out_recv,
+    kv_send, kv_recv, ctx_send, ctx_recv, away_send, away_recv, lane_send, lane_recv, set_send, set_recv,
+    head_send, head_recv, back_load, back_send, back_recv, out_send, out_recv,
 ):
     y, x, z, c = position()
     greet((sp_peer, tp_peer))
+    group = x // 2
+    right = c == group
+    wrong = c != group
+    partner = (y, 3 - x, z, 1 - c)
+    sibling = (y, x, z, 1 - c)
     wo_copy = pltpu.make_async_copy(wo, wo_v, back_load.at[0])
     own, stages, done, all_sent = gather_unit(kv, UNIT, kv_send, kv_recv)
-    ctx_own, ctx_stages, ctx_done, ctx_all_sent = gather_unit(ctx, 16, ctx_send, ctx_recv)
+    ctx_own, ctx_stages, ctx_done, ctx_all_sent = gather_unit(ctx, ROWS, ctx_send, ctx_recv)
+    settings[0, 0] = jnp.full((8, 128), lift[0] * LOG2E, F32)
+    settings[0, 1] = jnp.full((8, 128), lam[0], F32)
     peak[...] = jnp.full(peak.shape, -jnp.inf, F32)
     sums[...] = jnp.zeros(sums.shape, F32)
     acc[...] = jnp.zeros(acc.shape, F32)
-
-    def over(count, one, first=0):
-        lax.fori_loop(first, first + count, lambda o, carry: (one(o), carry)[1], 0)
+    there = lax.rem(3 - x, 2) * 4 + y
+    here = lax.rem(x, 2) * 4 + y
+
+    def early():
+        send(settings.at[0], settings.at[1], set_send.at[0], set_recv.at[0], sibling)
+
+    def away(*units):
+        @pl.when(wrong)
+        def _():
+            for o in units:
+                rows = pl.ds(o * UNIT, UNIT)
+                send(q.at[0, rows], q.at[1, rows], away_send.at[0], away_recv.at[NZ + 1], partner)
+                send(
+                    kv_away.at[o], kv.at[1 - c, o, pl.ds(pl.multiple_of(there * UNIT, UNIT), UNIT)],
+                    away_send.at[1], away_recv.at[o], partner,
+                )
+
+    def ctx_away_start():
+        @pl.when(wrong)
+        def _():
+            send(
+                ctx_away, ctx.at[1 - c, 0, pl.ds(pl.multiple_of(there * ROWS, ROWS), ROWS)],
+                away_send.at[2], away_recv.at[NZ], partner,
+            )
+
+    def begin(o):
+        @pl.when(wrong)
+        def _():
+            await_bytes(kv.at[0, 0, pl.ds(0, UNIT)], away_recv.at[o])
+
+        own(o)
+
+    def ctx_begin(o):
+        @pl.when(wrong)
+        def _():
+            await_bytes(ctx.at[0, 0, pl.ds(0, ROWS)], away_recv.at[NZ])
+
+        ctx_own(o)
+
+    def show_lane(o):
+        done(o)
+        send(kv.at[c, o], kv.at[c, o], lane_send.at[0], lane_recv.at[o], sibling)
+
+    def ctx_show_lane(o):
+        ctx_done(o)
+        send(ctx.at[c], ctx.at[c], lane_send.at[1], lane_recv.at[NZ], sibling)
+
+    choice = jnp.where(right, 0, 1)
+
+    def attend(m):
+        def one(o):
+            if m == 0:
+                await_bytes(kv.at[0, 0], lane_recv.at[o])
+            absorb(
+                q[choice, :, m * PART : (m + 1) * PART], m,
+                kv[:, o, :, m * PART : (m + 1) * PART].reshape(NS * UNIT, PART),
+                kv[:, o, :, HD : 2 * HD].reshape(NS * UNIT, HD), None, peak, sums, acc,
+            )
+
+        return one
+
+    def ctx_attend(o):
+        await_bytes(ctx.at[0], lane_recv.at[NZ])
+        lift_term = settings[choice, 0, 0:1, 0:1]
+        for m in range(2):
+            absorb(
+                q[choice, :, m * PART : (m + 1) * PART], m,
+                ctx[:, 0, :, m * PART : (m + 1) * PART].reshape(NS * ROWS, PART),
+                ctx[:, 0, :, HD : 2 * HD].reshape(NS * ROWS, HD), lift_term, peak, sums, acc,
+            )
+
+    steps = (
+        (3, stages[2]), (0, begin), (5, attend(0)), (4, show_lane), (1, stages[0]), (2, stages[1]), (5, attend(1)),
+    )
+    ctx_steps = {
+        1: ctx_begin, 2: ctx_stages[0], 3: ctx_stages[1], 4: ctx_stages[2], 5: ctx_show_lane, 6: ctx_attend,
+    }
+
+    def slot(t):
+        for after, one in steps:
+            o = t - after
+            if isinstance(t, int):
+                if 0 <= o < NZ:
+                    one(o)
+            else:
+
+                @pl.when((o >= 0) & (o < NZ))
+                def _(o=o, one=one):
+                    one(o)
+
+        for at, one in ctx_steps.items():
+            if isinstance(t, int):
+                if t == at:
+                    one(0)
+            elif at >= SLOTS_AHEAD[-1]:
+
+                @pl.when(t == at)
+                def _(one=one):
+                    one(0)
 
     def ahead(step):
         if step == 0:
-            own(0)
-            over(2, ctx_own)
+            away(0)
+            ctx_away_start()
             wo_copy.start()
+        else:
+            away(*((2 * step - 1, 2 * step) if step < 4 else (7,)))
+        for t in range(SLOTS_AHEAD[step], SLOTS_AHEAD[step + 1]):
+            slot(t)
         if step == 1:
-            over(2, own, 1)
-            over(2, ctx_stages[0])
-            stages[0](0)
             wo_copy.wait()
-            send(wo_v, wo_pair, back_send.at[1], back_recv.at[1], (y, x, z, 1 - c))
-        if step == 2:
-            over(2, own, 3)
-            over(2, ctx_stages[1])
-            stages[0](1)
-            stages[1](0)
-        if step == 3:
-            over(2, own, 5)
-            over(2, ctx_stages[2])
-            over(2, ctx_stages[3])
-            stages[0](2)
-            stages[1](1)
-            stages[2](0)
-        if step == 4:
-            own(7)
+            send(wo_v, wo_pair, back_send.at[1], back_recv.at[1], sibling)
 
     front(
         latent, context, cond, ctx_cond, modulation, wq, wk, wv, rcos, rsin, ccos, csin,
-        q, kv, ctx, mods, ahead,
+        q, kv, ctx, kv_away, ctx_away, mods, ahead, early,
         lat, wq_v, wk_v, wv_v, mod_v, ctx_v, parts, normed,
         load, mod_send, mod_recv, ring_send, ring_recv, pair_send, pair_recv,
     )
-    lift_term = lift[0] * LOG2E
-    lag = 5
-
-    def tick(t, carry):
-        def stage(k):
-            o = t - k
-
-            @pl.when((o >= 0) & (o < NZ))
-            def _():
-                stages[k](o)
-
-        def attend(m):
-            o = t - lag
-
-            @pl.when(o >= 0)
-            def _():
-                if m == 0:
-                    done(o)
-                absorb(q, m, kv[o, :, m * PART : (m + 1) * PART], kv[o, :, HD : 2 * HD], None, peak, sums, acc)
-
-        stage(0)
-        attend(0)
-        stage(1)
-        stage(2)
-        attend(1)
-        stage(3)
-
-        @pl.when(t == 3)
-        def _():
-            over(2, ctx_done)
-            for m in range(2):
-                absorb(
-                    q, m, ctx[:, :, m * PART : (m + 1) * PART].reshape(NS * ROWS, PART),
-                    ctx[:, :, HD : 2 * HD].reshape(NS * ROWS, HD), lift_term, peak, sums, acc,
-                )
-
+    await_bytes(settings.at[1], set_recv.at[0])
+
+    @pl.when(wrong)
+    def _():
+        await_bytes(q.at[1], away_recv.at[NZ + 1])
+
+    def later(t, carry):
+        slot(t)
         return carry
 
-    lax.fori_loop(3, NZ + lag, tick, 0)
+    lax.fori_loop(SLOTS_AHEAD[-1], NZ + 5, later, 0)
+    lam_term = settings[choice, 1, 0:1, 0:1]
     means = [acc[m] / sums[m][:, 0:1] for m in range(2)]
-    difference = means[0] - lam[0] * means[1]
+    difference = means[0] - lam_term * means[1]
     spread = jnp.mean(difference * difference, axis=1, keepdims=True)
-    final = (difference * lax.rsqrt(spread + EPS) * gain[...]).astype(BF16)
-    attended[0] = final[0:HD]
-    attended[1] = final[HD : 2 * HD]
+    final = (difference * lax.rsqrt(spread + EPS) * gain[...]).astype(BF16).reshape(NZ, 2, ROWS, HD)
+    for core in (0, 1):
+        attended[core] = final[:, core].reshape(HD, HD)
+
+    @pl.when(right)
+    def _():
+        heads[0] = attended[c]
+        send(attended.at[1 - c], heads.at[1], head_send.at[0], head_recv.at[0], sibling)
+        await_bytes(heads.at[0], head_recv.at[1])
+
+    @pl.when(wrong)
+    def _():
+        for core in (0, 1):
+            slot = jnp.where(c == core, 1, 0)
+            send(
+                attended.at[core], heads.at[slot], head_send.at[core], head_recv.at[1], (y, 3 - x, z, core)
+            )
+        await_bytes(heads.at[0], head_recv.at[0])
+        await_bytes(heads.at[0], head_recv.at[1])
+
     back(
-        attended, lat, mods, result, theirs, wo_v, wo_pair, part, out_buf, in_buf,
+        heads, lat, mods, result, wo_v, wo_pair, part, out_buf, in_buf,
         back_send, back_recv, out_send, out_recv,
     )
-    all_sent()
-    ctx_all_sent()
+    all_sent(NZ)
+    ctx_all_sent(1)
+    await_bytes(settings.at[0], set_send.at[0])
+    await_bytes(ctx.at[0], lane_send.at[1])
+    for o in range(NZ):
+        await_bytes(kv.at[0, 0], lane_send.at[0])
+    await_bytes(heads.at[0], head_send.at[0])
+
+    @pl.when(wrong)
+    def _():
+        await_bytes(heads.at[0], head_send.at[1])
+        await_bytes(q.at[0], away_send.at[0])
+        await_bytes(kv_away, away_send.at[1])
+        await_bytes(ctx_away, away_send.at[2])
 
 
 def run(*arrays):
@@ -562,14 +693,17 @@
             pltpu.VMEM((NS, 8, HD), F32),
             pltpu.VMEM((2 * UNIT, D), BF16),
             pltpu.VMEM((8, D), F32),
-            pltpu.VMEM((BLOCK, HD), BF16),
-            pltpu.VMEM((NZ, NS * UNIT, 2 * HD), BF16),
-            pltpu.VMEM((2, NS * 16, 2 * HD), BF16),
+            pltpu.VMEM((2, BLOCK, HD), BF16),
+            pltpu.VMEM((2, NZ, NS // 2 * UNIT, 2 * HD), BF16),
+            pltpu.VMEM((2, 1, NS // 2 * ROWS, 2 * HD), BF16),
+            pltpu.VMEM((NZ, UNIT, 2 * HD), BF16),
+            pltpu.VMEM((ROWS, 2 * HD), BF16),
+            pltpu.VMEM((2, 2, 8, 128), F32),
             pltpu.VMEM((2, BLOCK, 128), F32),
             pltpu.VMEM((2, BLOCK, 128), F32),
             pltpu.VMEM((2, BLOCK, HD), F32),
             pltpu.VMEM((2, HD, HD), BF16),
-            pltpu.VMEM((HD, HD), BF16),
+            pltpu.VMEM((2, HD, HD), BF16),
             pltpu.VMEM((HD, D), BF16),
             pltpu.VMEM((HD, D), BF16),
             pltpu.VMEM((CHUNKS, NZ, ROWS, WIDE), F32),
@@ -583,9 +717,17 @@
             dma((NZ,)),
             dma((NZ,)),
             dma((1,)),
-            dma((5 * NZ,)),
+            dma((4 * NZ,)),
             dma((1,)),
-            dma((10,)),
+            dma((4,)),
+            dma((3,)),
+            dma((NZ + 2,)),
+            dma((2,)),
+            dma((NZ + 1,)),
+            dma((1,)),
+            dma((1,)),
+            dma((2,)),
+            dma((2,)),
             dma((1,)),
             dma((2,)),
             dma((2,)),

time: 121 us -> 115 us (0.950)
  Pallas kernels: 118 us -> 112 us
    pallas_call x1, Pallas kernels: 118 us -> 112 us  [run(): pl.pallas_call(kernel, out_shape=jax.ShapeDtypeStruct((ROWS, D), BF16), i...]
where the time goes in v3:
time: 115 us
  Pallas kernels  112 us (97%)
  local copies, waits for them, and re-layouts  1.67 us (1%)
  between operations  1.31 us (1%)
    pallas_call x1, Pallas kernels, run(): pl.pallas_call(kernel, out_shape=jax.ShapeDtypeStruct((ROWS, D), BF16), i...  112 us

profile of v3, /device:TPU:1, one launch (start us, length us, event | category | flops | bytes accessed | tf_op | source)
XLA Modules:
  0.0 115.3 jit_solution(17744194488593166217)
XLA Ops:
  1.3 112.3 %whole.1 = bf16[32,4096]{1,0:T(8,128)(2,1)} custom-call(bf16[32,4096]{1,0:T(8,128)(2,1)} %latent.1, bf16[32,4096]{1,0:T(8,128)(2,1)} %context.1, f32[32,128]{1,0:T(8,128)} %bitcast.3, f32[32,128]{1,0:T(8,128)} %bitcast.4, bf16[3,256,256]{2,1,0:T(8,128)(2,1)} %modulation.1, bf16[4096,256]{1,0:T(8,128)(2,1)} %wq.1, bf16[4096,256]{1,0:T(8,128)(2,1)} %wk.1, ...), custom_call_target="tpu_custom_call" | custom-call | tf_op jit(solution)/shard_map/whole/pallas_call | solution.py:681
  113.6 1.7 %copy.20 = bf16[32,4096]{1,0:T(8,128)(2,1)} copy(bf16[32,4096]{1,0:T(8,128)(2,1)} %whole.1) | data formatting | bytes 524288

commit v4 on v3

--- a/solution.py
+++ b/solution.py
@@ -391,20 +391,23 @@
     return own, (stage1, stage2, stage3), done, all_sent
 
 
-def absorb(q, m, keys, values, lift, peak, sums, acc):
-    scores = lax.dot_general(
-        q, keys, (((1,), (1,)), ((), ())), preferred_element_type=F32
-    )
-    scores = scores * (PART**-0.5 * LOG2E)
-    if lift is not None:
-        scores = scores + lift
-    before = peak[m]
-    now = jnp.maximum(before, jnp.max(scores, axis=1, keepdims=True))
-    fading = jnp.exp2(before - now)
-    weights = jnp.exp2(scores - now[:, 0:1])
-    sums[m] = sums[m] * fading + jnp.sum(weights, axis=1, keepdims=True)
-    acc[m] = acc[m] * fading[:, 0:1] + jnp.dot(weights.astype(BF16), values, preferred_element_type=F32)
-    peak[m] = now
+def absorb(q, slot, rows, keys, values, lift, peak, sums, acc):
+    for m in range(2):
+        scores = lax.dot_general(
+            q[slot, rows, m * PART : (m + 1) * PART], keys(m), (((1,), (1,)), ((), ())), preferred_element_type=F32
+        )
+        scores = scores * (PART**-0.5 * LOG2E)
+        if lift is not None:
+            scores = scores + lift
+        before = peak[m, rows]
+        now = jnp.maximum(before, jnp.max(scores, axis=1, keepdims=True))
+        fading = jnp.exp2(before - now)
+        weights = jnp.exp2(scores - now[:, 0:1])
+        sums[m, rows] = sums[m, rows] * fading + jnp.sum(weights, axis=1, keepdims=True)
+        acc[m, rows] = acc[m, rows] * fading[:, 0:1] + jnp.dot(
+            weights.astype(BF16), values(), preferred_element_type=F32
+        )
+        peak[m, rows] = now
 
 
 CHUNKS = 4
@@ -550,27 +553,56 @@
 
     choice = jnp.where(right, 0, 1)
 
-    def attend(m):
+    half = BLOCK // 2
+
+    def attend(r):
+        rows = slice(r * half, (r + 1) * half)
+
         def one(o):
-            if m == 0:
+            if r == 0:
                 await_bytes(kv.at[0, 0], lane_recv.at[o])
             absorb(
-                q[choice, :, m * PART : (m + 1) * PART], m,
-                kv[:, o, :, m * PART : (m + 1) * PART].reshape(NS * UNIT, PART),
-                kv[:, o, :, HD : 2 * HD].reshape(NS * UNIT, HD), None, peak, sums, acc,
+                q, choice, rows,
+                lambda m: kv[:, o, :, m * PART : (m + 1) * PART].reshape(NS * UNIT, PART),
+                lambda: kv[:, o, :, HD : 2 * HD].reshape(NS * UNIT, HD), None, peak, sums, acc,
             )
+            pl.when(o == NZ - 1)(functools.partial(finish, r))
 
         return one
 
     def ctx_attend(o):
         await_bytes(ctx.at[0], lane_recv.at[NZ])
         lift_term = settings[choice, 0, 0:1, 0:1]
-        for m in range(2):
+        for r in range(2):
             absorb(
-                q[choice, :, m * PART : (m + 1) * PART], m,
-                ctx[:, 0, :, m * PART : (m + 1) * PART].reshape(NS * ROWS, PART),
-                ctx[:, 0, :, HD : 2 * HD].reshape(NS * ROWS, HD), lift_term, peak, sums, acc,
+                q, choice, slice(r * half, (r + 1) * half),
+                lambda m: ctx[:, 0, :, m * PART : (m + 1) * PART].reshape(NS * ROWS, PART),
+                lambda: ctx[:, 0, :, HD : 2 * HD].reshape(NS * ROWS, HD), lift_term, peak, sums, acc,
             )
+
+    def finish(r):
+        rows = slice(r * half, (r + 1) * half)
+        means = [acc[m, rows] / sums[m, rows][:, 0:1] for m in range(2)]
+        difference = means[0] - settings[choice, 1, 0:1, 0:1] * means[1]
+        spread = jnp.mean(difference * difference, axis=1, keepdims=True)
+        final = (difference * lax.rsqrt(spread + EPS) * gain[...]).astype(BF16).reshape(NZ // 2, 2, ROWS, HD)
+        ours = slice(r * half // 2, (r + 1) * half // 2)
+        for core in (0, 1):
+            attended[core, ours] = final[:, core].reshape(half // 2, HD)
+
+        @pl.when(right)
+        def _():
+            heads[0, ours] = attended[c, ours]
+            send(attended.at[1 - c, ours], heads.at[1, ours], head_send.at[2 * r], head_recv.at[r], sibling)
+
+        @pl.when(wrong)
+        def _():
+            for core in (0, 1):
+                slot = jnp.where(c == core, 1, 0)
+                send(
+                    attended.at[core, ours], heads.at[slot, ours], head_send.at[2 * r + core], head_recv.at[2 + r],
+                    (y, 3 - x, z, core),
+                )
 
     steps = (
         (3, stages[2]), (0, begin), (5, attend(0)), (4, show_lane), (1, stages[0]), (2, stages[1]), (5, attend(1)),
@@ -631,29 +663,13 @@
         return carry
 
     lax.fori_loop(SLOTS_AHEAD[-1], NZ + 5, later, 0)
-    lam_term = settings[choice, 1, 0:1, 0:1]
-    means = [acc[m] / sums[m][:, 0:1] for m in range(2)]
-    difference = means[0] - lam_term * means[1]
-    spread = jnp.mean(difference * difference, axis=1, keepdims=True)
-    final = (difference * lax.rsqrt(spread + EPS) * gain[...]).astype(BF16).reshape(NZ, 2, ROWS, HD)
-    for core in (0, 1):
-        attended[core] = final[:, core].reshape(HD, HD)
-
-    @pl.when(right)
-    def _():
-        heads[0] = attended[c]
-        send(attended.at[1 - c], heads.at[1], head_send.at[0], head_recv.at[0], sibling)
-        await_bytes(heads.at[0], head_recv.at[1])
-
-    @pl.when(wrong)
-    def _():
-        for core in (0, 1):
-            slot = jnp.where(c == core, 1, 0)
-            send(
-                attended.at[core], heads.at[slot], head_send.at[core], head_recv.at[1], (y, 3 - x, z, core)
-            )
-        await_bytes(heads.at[0], head_recv.at[0])
-        await_bytes(heads.at[0], head_recv.at[1])
+    some = heads.at[0, pl.ds(0, half // 2)]
+    for r in range(2):
+        await_bytes(some, head_recv.at[2 + r])
+
+        @pl.when(wrong)
+        def _(r=r):
+            await_bytes(some, head_recv.at[r])
 
     back(
         heads, lat, mods, result, wo_v, wo_pair, part, out_buf, in_buf,
@@ -665,11 +681,13 @@
     await_bytes(ctx.at[0], lane_send.at[1])
     for o in range(NZ):
         await_bytes(kv.at[0, 0], lane_send.at[0])
-    await_bytes(heads.at[0], head_send.at[0])
+    for r in range(2):
+        await_bytes(some, head_send.at[2 * r])
 
     @pl.when(wrong)
     def _():
-        await_bytes(heads.at[0], head_send.at[1])
+        for r in range(2):
+            await_bytes(some, head_send.at[2 * r + 1])
         await_bytes(q.at[0], away_send.at[0])
         await_bytes(kv_away, away_send.at[1])
         await_bytes(ctx_away, away_send.at[2])
@@ -726,8 +744,8 @@
             dma((NZ + 1,)),
             dma((1,)),
             dma((1,)),
-            dma((2,)),
-            dma((2,)),
+            dma((4,)),
+            dma((4,)),
             dma((1,)),
             dma((2,)),
             dma((2,)),

time: 115 us -> 110 us (0.957)
  Pallas kernels: 112 us -> 107 us
    pallas_call x1, Pallas kernels: 112 us -> 107 us  [run(): pl.pallas_call(kernel, out_shape=jax.ShapeDtypeStruct((ROWS, D), BF16), i...]
where the time goes in v4:
time: 110 us
  Pallas kernels  107 us (97%)
  local copies, waits for them, and re-layouts  1.67 us (2%)
  between operations  1.31 us (1%)
    pallas_call x1, Pallas kernels, run(): pl.pallas_call(kernel, out_shape=jax.ShapeDtypeStruct((ROWS, D), BF16), i...  107 us

profile of v4, /device:TPU:1, one launch (start us, length us, event | category | flops | bytes accessed | tf_op | source)
XLA Modules:
  0.0 109.9 jit_solution(17734872466803641334)
XLA Ops:
  1.3 107.0 %whole.1 = bf16[32,4096]{1,0:T(8,128)(2,1)} custom-call(bf16[32,4096]{1,0:T(8,128)(2,1)} %latent.1, bf16[32,4096]{1,0:T(8,128)(2,1)} %context.1, f32[32,128]{1,0:T(8,128)} %bitcast.3, f32[32,128]{1,0:T(8,128)} %bitcast.4, bf16[3,256,256]{2,1,0:T(8,128)(2,1)} %modulation.1, bf16[4096,256]{1,0:T(8,128)(2,1)} %wq.1, bf16[4096,256]{1,0:T(8,128)(2,1)} %wk.1, ...), custom_call_target="tpu_custom_call" | custom-call | tf_op jit(solution)/shard_map/whole/pallas_call | solution.py:699
  108.3 1.7 %copy.20 = bf16[32,4096]{1,0:T(8,128)(2,1)} copy(bf16[32,4096]{1,0:T(8,128)(2,1)} %whole.1) | data formatting | bytes 524288

commit v5 on v4

--- a/solution.py
+++ b/solution.py
@@ -270,11 +270,11 @@
     pair_wait(0)
     project([0], True)
     ahead(0)
+    forward(3)
     for rel in (7, 1):
         pair_wait(rel)
     project([7, 1], False)
     ahead(1)
-    forward(3)
     for rel in (6, 2):
         pair_wait(rel)
     project([6, 2], False)

time: 110 us -> 114 us (1.036)
  Pallas kernels: 107 us -> 110 us
    pallas_call x1, Pallas kernels: 107 us -> 110 us  [run(): pl.pallas_call(kernel, out_shape=jax.ShapeDtypeStruct((ROWS, D), BF16), i...]
where the time goes in v5:
time: 114 us; the launch traced here: 113 us
  Pallas kernels  110 us (96%)
  local copies, waits for them, and re-layouts  1.67 us (1%)
  between operations  1.31 us (1%)
    pallas_call x1, Pallas kernels, run(): pl.pallas_call(kernel, out_shape=jax.ShapeDtypeStruct((ROWS, D), BF16), i...  110 us

profile of v5, /device:TPU:1, one launch (start us, length us, event | category | flops | bytes accessed | tf_op | source)
XLA Modules:
  0.0 113.4 jit_solution(1197680817731387081)
XLA Ops:
  1.3 110.5 %whole.1 = bf16[32,4096]{1,0:T(8,128)(2,1)} custom-call(bf16[32,4096]{1,0:T(8,128)(2,1)} %latent.1, bf16[32,4096]{1,0:T(8,128)(2,1)} %context.1, f32[32,128]{1,0:T(8,128)} %bitcast.3, f32[32,128]{1,0:T(8,128)} %bitcast.4, bf16[3,256,256]{2,1,0:T(8,128)(2,1)} %modulation.1, bf16[4096,256]{1,0:T(8,128)(2,1)} %wq.1, bf16[4096,256]{1,0:T(8,128)(2,1)} %wk.1, ...), custom_call_target="tpu_custom_call" | custom-call | tf_op jit(solution)/shard_map/whole/pallas_call | solution.py:699
  111.8 1.7 %copy.20 = bf16[32,4096]{1,0:T(8,128)(2,1)} copy(bf16[32,4096]{1,0:T(8,128)(2,1)} %whole.1) | data formatting | bytes 524288
